TPU v7x, 32 devices: a whole 2x2x4 slice. The times are simulated.
32 devices in a mesh: grp: 2 (over x), sp: 4 (over y, core), tp: 4 (over z).
Axes of the slice: x: 2, y: 2, z: 4, core: 2. Of those that a mesh axis runs over, the one named last changes fastest.
Arguments:
- residual: bfloat16 [4096, 2048], P(('grp', 'sp', 'tp')), parts along dimension 0, may hold values from -6 to 6
- grouped_value_heads: bfloat16 [4096, 2, 1024], P(('grp', 'sp'), None, 'tp'), parts along dimension 0, may hold values from -6 to 6
- output_gate_heads: bfloat16 [4096, 2, 1024], P(('grp', 'sp'), None, 'tp'), parts along dimension 0, may hold values from -6 to 6
- projected_key_query: bfloat16 [4096, 384], P(('grp', 'sp')), parts along dimension 0, may hold values from -6 to 6
- raw_step_size: bfloat16 [4096, 2, 16], P(('grp', 'sp'), None, 'tp'), parts along dimension 0, may hold values from -3 to 3
- step_size_bias: float32 [2, 16], P(None, 'tp'), may hold values from -1 to 0.5
- head_decay_logarithm: float32 [2, 16], P(None, 'tp'), may hold values from -16 to -2
- position_extra_decay: float32 [4096], P(('grp', 'sp')), parts along dimension 0, may hold values from -0.7 to 0
- head_skip_weight: float32 [2, 16], P(None, 'tp'), may hold values from 0.5 to 2
- value_kernel_taps: bfloat16 [4, 2, 1024], P(None, None, 'tp'), may hold values from -3 to 3
- key_query_kernel: bfloat16 [4, 384], replicated, may hold values from -3 to 3
- head_norm_gain: float32 [2, 1024], P(None, 'tp'), may hold values from 0.1 to 1.9
- output_matrix: bfloat16 [2, 1024, 2048], P(None, 'tp'), may hold values from -0.125 to 0.125
- expert_norm_gain: float32 [2048], replicated, may hold values from 0.1 to 1.9
- expert_gate_weight: bfloat16 [4, 2048, 4096], P('sp', None, 'tp'), may hold values from -0.125 to 0.125
- expert_up_weight: bfloat16 [4, 2048, 4096], P('sp', None, 'tp'), may hold values from -0.125 to 0.125
- expert_down_weight: bfloat16 [4, 4096, 2048], P('sp', 'tp'), may hold values from -0.09375 to 0.09375
- token_expert_choice: int32 [4096, 2], P(('grp', 'sp', 'tp')), parts along dimension 0, may hold values from 0 to 3, all different within a row; in each aligned block of 128 rows (0 to 127, 128 to 255, ...) at most 65 rows name the same one
- expert_output_weight: float32 [4096, 2], P(('grp', 'sp', 'tp')), parts along dimension 0, may hold values from 0.2 to 1
Outputs:
- layer_out: bfloat16 [4096, 2048], P(('grp', 'sp', 'tp')), parts along dimension 0
There are 2 independent parts, one for each index of `grp`. A program takes and returns all parts, laid end to end along the dimension named above; an argument that names none is the same for every part. Nothing has to cross between parts.
Inputs may be any that keep to these rules, and one draw needn't show every extreme that they name: `token_expert_choice`: each row names two different experts. The token rows of one device name one expert at most 65 times.
All inputs are finite; a program needn't handle non-finite values.
Results may differ from a plain program's by a relative error of at most 0.015.
Values may be sent and summed in bfloat16 or wider, within the bound.
No kernel may reach another device: no remote copies, remote signals or barrier semaphores. Data moves between devices by JAX's collectives and lax.ppermute only.
A program may use at most 128 MiB of HBM per device.

v0:
```python
import functools

import jax
import jax.numpy as jnp
from jax import lax
from jax.experimental import pallas as pl
from jax.experimental.pallas import tpu as pltpu
from jax.sharding import PartitionSpec as P


HEAD_DIM = 64
STATE_ONE = 64
STATE_TWO = 128
BLOCK = 128


EPSILON = 1e-06


def passed_along(shard, axis, by):
    length = lax.axis_size(axis)
    pairs = [(i, i + by) for i in range(length) if 0 <= i + by < length]
    return lax.ppermute(shard, axis, pairs)


def high_rows(heads):
    return -(-2 * heads // 8) * 8


def widened(column, heads, width):
    rows = column.shape[0]
    return jnp.concatenate(
        [jnp.broadcast_to(column[:, h : h + 1], (rows, width)) for h in range(heads)], axis=1
    )


def spread_down(tall, first, heads, width):
    return jnp.concatenate(
        [jnp.broadcast_to(tall[first + h : first + h + 1], (1, width)) for h in range(heads)], axis=1
    )


def both_groups(tall, heads, width):
    return jnp.concatenate(
        [spread_down(tall, g * heads, heads, width) for g in range(2)], axis=1
    )


def states_kernel(
    heads,
    sizes,
    values_ref,
    keys_ref,
    rim_ref,
    value_taps_ref,
    key_taps_ref,
    steps_ref,
    facts_ref,
    extra_ref,
    x_ref,
    rows_ref,
    across_ref,
    down_ref,
    enter_one_ref,
    enter_two_ref,
    earlier_ref,
    packed_ref,
    tail_ref,
    one_ref,
    two_ref,
    sum_ref,
):
    step = pl.program_id(0)
    lanes = heads * HEAD_DIM
    taps = value_taps_ref.shape[0]

    @pl.when(step == 0)
    def _():
        tail_ref[...] = rim_ref[...].astype(jnp.float32)
        one_ref[...] = jnp.zeros_like(one_ref)
        two_ref[...] = jnp.zeros_like(two_ref)
        sum_ref[...] = jnp.zeros_like(sum_ref)

    here = jnp.concatenate(
        [values_ref[...].astype(jnp.float32), keys_ref[...].astype(jnp.float32)], axis=1
    )
    extended = jnp.concatenate([tail_ref[...], here], axis=0)
    tail_ref[...] = here[BLOCK - 8 :]
    weights = jnp.concatenate(
        [value_taps_ref[...].astype(jnp.float32), key_taps_ref[...].astype(jnp.float32)], axis=1
    )
    summed = jnp.zeros_like(here)
    for j in range(taps):
        first = 8 - (taps - 1) + j
        summed = summed + extended[first : first + BLOCK] * weights[j : j + 1]
    active = (summed * jax.nn.sigmoid(summed)).astype(jnp.bfloat16)
    x = active[:, : 2 * lanes]
    rows = active[:, 2 * lanes :]
    x_ref[...] = x
    rows_ref[...] = rows

    raw = steps_ref[...] + facts_ref[:, 0:1]
    stride = jnp.maximum(raw, 0.0) + jnp.log1p(jnp.exp(-jnp.abs(raw)))
    log_decay = extra_ref[...] - jnp.exp(facts_ref[:, 1:2]) * stride
    upto = (
        lax.broadcasted_iota(jnp.int32, (BLOCK, BLOCK), 0)
        <= lax.broadcasted_iota(jnp.int32, (BLOCK, BLOCK), 1)
    ).astype(jnp.float32)
    running = jnp.dot(
        log_decay, upto, preferred_element_type=jnp.float32, precision=lax.Precision.HIGHEST
    )
    end = running[:, BLOCK - 1 :]
    fading = jnp.exp(end - running) * stride
    high = running.shape[0]
    stacked = jnp.concatenate(
        [running, fading, jnp.exp(running)]
        + [jnp.zeros((BLOCK - 3 * high, BLOCK), jnp.float32)],
        axis=0,
    )
    down = stacked.T
    across_ref[...] = jnp.concatenate([running, stride], axis=0)
    down_ref[...] = down
    earlier_ref[...] = jnp.broadcast_to(
        jnp.exp(both_groups(sum_ref[...], heads, HEAD_DIM)), earlier_ref.shape
    )
    faded_end = jnp.exp(both_groups(end, heads, HEAD_DIM))
    bound = 0
    for g, (enter_ref, state_ref) in enumerate(((enter_one_ref, one_ref), (enter_two_ref, two_ref))):
        keys = rows[:, bound : bound + sizes[g]]
        bound += 2 * sizes[g]
        fade = widened(down[:, high + g * heads : high + (g + 1) * heads], heads, HEAD_DIM)
        scaled = (x[:, g * lanes : (g + 1) * lanes].astype(jnp.float32) * fade).astype(jnp.bfloat16)
        own = lax.dot_general(
            keys, scaled, (((0,), (0,)), ((), ())), preferred_element_type=jnp.float32
        )
        state = state_ref[...]
        enter_ref[0] = state
        state_ref[...] = state * faded_end[:, g * lanes : (g + 1) * lanes] + own
    total = sum_ref[...] + end
    sum_ref[...] = total

    @pl.when(step == pl.num_programs(0) - 1)
    def _():
        whole = both_groups(total, heads, HEAD_DIM)
        high_part = whole.astype(jnp.bfloat16)
        low_part = (whole - high_part.astype(jnp.float32)).astype(jnp.bfloat16)
        packed_ref[0 : sizes[0]] = one_ref[...].astype(jnp.bfloat16)
        packed_ref[sizes[0] : sizes[0] + sizes[1]] = two_ref[...].astype(jnp.bfloat16)
        packed_ref[sizes[0] + sizes[1] :] = jnp.concatenate(
            [
                jnp.broadcast_to(part[:, g * lanes : (g + 1) * lanes].astype(jnp.float32), (4, lanes))
                for g in range(2)
                for part in (high_part, low_part)
            ],
            axis=0,
        ).astype(jnp.bfloat16)


def near_kernel(heads, sizes, x_ref, rows_ref, across_ref, down_ref, facts_ref, near_ref):
    high = across_ref.shape[0] // 2
    later = lax.broadcasted_iota(jnp.int32, (BLOCK, BLOCK), 0) >= lax.broadcasted_iota(
        jnp.int32, (BLOCK, BLOCK), 1
    )
    skip = both_groups(facts_ref[:, 2:3], heads, HEAD_DIM)
    bound = 0
    out = []
    for g in range(2):
        keys = rows_ref[:, bound : bound + sizes[g]]
        queries = rows_ref[:, bound + sizes[g] : bound + 2 * sizes[g]]
        bound += 2 * sizes[g]
        scores = lax.dot_general(
            queries, keys, (((1,), (1,)), ((), ())), preferred_element_type=jnp.float32
        )
        for h in range(heads):
            i = g * heads + h
            spread = jnp.where(later, down_ref[:, i : i + 1] - across_ref[i : i + 1], -1e30)
            weights = scores * jnp.exp(spread) * across_ref[high + i : high + i + 1]
            x = x_ref[:, i * HEAD_DIM : (i + 1) * HEAD_DIM]
            out.append(
                jnp.dot(weights.astype(jnp.bfloat16), x, preferred_element_type=jnp.float32)
            )
    near_ref[...] = jnp.concatenate(out, axis=1) + skip * x_ref[...].astype(jnp.float32)


def mixed_values(heads, sizes, prior_count, refs):
    priors = refs[:prior_count]
    (
        near_ref,
        rows_ref,
        down_ref,
        enter_one_ref,
        enter_two_ref,
        earlier_ref,
        gate_ref,
        gain_ref,
        one_ref,
        two_ref,
    ) = refs[prior_count:]
    lanes = heads * HEAD_DIM
    high = high_rows(heads)

    @pl.when(pl.program_id(0) == 0)
    def _():
        base = sizes[0] + sizes[1]
        for g, state_ref in enumerate((one_ref, two_ref)):
            state = jnp.zeros_like(state_ref)
            first = g * sizes[0]
            for prior in reversed(priors):
                facts = prior[base:].astype(jnp.float32)
                decay = facts[8 * g : 8 * g + 1] + facts[8 * g + 4 : 8 * g + 5]
                own = prior[first : first + sizes[g]].astype(jnp.float32)
                state = state * jnp.exp(decay) + own
            state_ref[...] = state

    bound = 0
    out = []
    for g, (enter_ref, state_ref) in enumerate(((enter_one_ref, one_ref), (enter_two_ref, two_ref))):
        queries = rows_ref[:, bound + sizes[g] : bound + 2 * sizes[g]]
        bound += 2 * sizes[g]
        here = slice(g * lanes, (g + 1) * lanes)
        entering = enter_ref[0] + state_ref[...] * earlier_ref[0:1, here]
        far = jnp.dot(
            queries, entering.astype(jnp.bfloat16), preferred_element_type=jnp.float32
        )
        reach = down_ref[:, 2 * high + g * heads : 2 * high + (g + 1) * heads]
        gate = gate_ref[:, here].astype(jnp.float32)
        total = near_ref[:, here] + far * widened(reach, heads, HEAD_DIM)
        gated = total * (gate * jax.nn.sigmoid(gate))
        squares = gated * gated
        means = jnp.concatenate(
            [
                jnp.sum(squares[:, h * HEAD_DIM : (h + 1) * HEAD_DIM], axis=1, keepdims=True)
                for h in range(heads)
            ],
            axis=1,
        ) * (1.0 / HEAD_DIM)
        scale = widened(lax.rsqrt(means + EPSILON), heads, HEAD_DIM)
        out.append((gated * scale * gain_ref[:, here]).astype(jnp.bfloat16))
    return jnp.concatenate(out, axis=1)


def mixed_kernel(heads, sizes, prior_count, *refs):
    inputs = prior_count + 8
    refs[inputs][...] = mixed_values(heads, sizes, prior_count, refs[:inputs] + refs[inputs + 1 :])


def projected_kernel(heads, sizes, prior_count, turns, order_ref, *refs):
    inputs = prior_count + 8
    matrix_ref, outs = refs[inputs], refs[inputs + 1 : inputs + 1 + turns]
    mixed = mixed_values(heads, sizes, prior_count, refs[:inputs] + refs[inputs + 1 + turns :])
    product = jnp.dot(mixed, matrix_ref[...], preferred_element_type=jnp.float32)
    for turn, out_ref in enumerate(outs):

        @pl.when(pl.program_id(0) == turn)
        def _(out_ref=out_ref):
            out_ref[...] = product.astype(jnp.bfloat16)


def mixed_rows(
    grouped_value_heads,
    output_gate_heads,
    projected_key_query,
    raw_step_size,
    step_size_bias,
    head_decay_logarithm,
    position_extra_decay,
    head_skip_weight,
    value_kernel_taps,
    key_query_kernel,
    head_norm_gain,
    output_matrix,
    order,
):
    positions, _, lanes = grouped_value_heads.shape
    heads = lanes // HEAD_DIM
    high = high_rows(heads)
    sizes = (STATE_ONE, STATE_TWO)
    width = key_query_kernel.shape[1]
    blocks = positions // BLOCK
    last = grouped_value_heads[positions - 8 :].reshape(8, 2 * lanes)
    rim = passed_along(
        jnp.concatenate([last, projected_key_query[positions - 8 :]], axis=1), "sp", 1
    )
    values = grouped_value_heads.reshape(positions, 2 * lanes)
    facts = jnp.stack(
        [step_size_bias.reshape(-1), head_decay_logarithm.reshape(-1), head_skip_weight.reshape(-1)],
        axis=1,
    )
    facts = jnp.pad(facts, ((0, high - 2 * heads), (0, 0)))
    steps = raw_step_size.reshape(positions, 2 * heads).T.astype(jnp.float32)
    steps = jnp.pad(steps, ((0, high - 2 * heads), (0, 0)))

    def by_block(rows, columns):
        return pl.BlockSpec((rows, columns), lambda k: (k, 0))

    def along(rows):
        return pl.BlockSpec((rows, BLOCK), lambda k: (0, k))

    def fixed(*shape):
        return pl.BlockSpec(shape, lambda k: (0,) * len(shape))

    def per_block(*shape):
        return pl.BlockSpec((1, *shape), lambda k: (k,) + (0,) * len(shape))

    f32, bf16 = jnp.float32, jnp.bfloat16
    packed_rows = sizes[0] + sizes[1] + 16
    x, rows, across, down, enter_one, enter_two, earlier, packed = pl.pallas_call(
        functools.partial(states_kernel, heads, sizes),
        grid=(blocks,),
        in_specs=[
            by_block(BLOCK, 2 * lanes),
            by_block(BLOCK, width),
            fixed(8, 2 * lanes + width),
            fixed(value_kernel_taps.shape[0], 2 * lanes),
            fixed(*key_query_kernel.shape),
            along(high),
            fixed(high, 3),
            along(1),
        ],
        out_specs=[
            by_block(BLOCK, 2 * lanes),
            by_block(BLOCK, width),
            along(2 * high),
            by_block(BLOCK, BLOCK),
            per_block(sizes[0], lanes),
            per_block(sizes[1], lanes),
            by_block(8, 2 * lanes),
            fixed(packed_rows, lanes),
        ],
        out_shape=[
            jax.ShapeDtypeStruct((positions, 2 * lanes), bf16),
            jax.ShapeDtypeStruct((positions, width), bf16),
            jax.ShapeDtypeStruct((2 * high, positions), f32),
            jax.ShapeDtypeStruct((positions, BLOCK), f32),
            jax.ShapeDtypeStruct((blocks, sizes[0], lanes), f32),
            jax.ShapeDtypeStruct((blocks, sizes[1], lanes), f32),
            jax.ShapeDtypeStruct((8 * blocks, 2 * lanes), f32),
            jax.ShapeDtypeStruct((packed_rows, lanes), bf16),
        ],
        scratch_shapes=[
            pltpu.VMEM((8, 2 * lanes + width), f32),
            pltpu.VMEM((sizes[0], lanes), f32),
            pltpu.VMEM((sizes[1], lanes), f32),
            pltpu.VMEM((high, 1), f32),
        ],
        name="states",
    )(
        values,
        projected_key_query,
        rim,
        value_kernel_taps.reshape(-1, 2 * lanes),
        key_query_kernel,
        steps,
        facts,
        position_extra_decay[None],
    )
    priors = [passed_along(packed, "sp", by) for by in range(1, lax.axis_size("sp"))]
    near = pl.pallas_call(
        functools.partial(near_kernel, heads, sizes),
        grid=(blocks,),
        in_specs=[
            by_block(BLOCK, 2 * lanes),
            by_block(BLOCK, width),
            along(2 * high),
            by_block(BLOCK, BLOCK),
            fixed(high, 3),
        ],
        out_specs=by_block(BLOCK, 2 * lanes),
        out_shape=jax.ShapeDtypeStruct((positions, 2 * lanes), f32),
        name="near",
    )(x, rows, across, down, facts)
    operands = (
        *priors,
        near,
        rows,
        down,
        enter_one,
        enter_two,
        earlier,
        output_gate_heads.reshape(positions, 2 * lanes),
        head_norm_gain.reshape(1, 2 * lanes),
    )
    scratch_shapes = [pltpu.VMEM((sizes[0], lanes), f32), pltpu.VMEM((sizes[1], lanes), f32)]
    if order is None:
        return pl.pallas_call(
            functools.partial(mixed_kernel, heads, sizes, len(priors)),
            grid=(blocks,),
            in_specs=[fixed(packed_rows, lanes) for _ in priors]
            + [
                by_block(BLOCK, 2 * lanes),
                by_block(BLOCK, width),
                by_block(BLOCK, BLOCK),
                per_block(sizes[0], lanes),
                per_block(sizes[1], lanes),
                by_block(8, 2 * lanes),
                by_block(BLOCK, 2 * lanes),
                fixed(1, 2 * lanes),
            ],
            out_specs=by_block(BLOCK, 2 * lanes),
            out_shape=jax.ShapeDtypeStruct((positions, 2 * lanes), bf16),
            scratch_shapes=scratch_shapes,
            name="mixed",
        )(*operands)

    def whole(*shape):
        return pl.BlockSpec(shape, lambda k, order: (0,) * len(shape))

    def chosen(rows, columns):
        return pl.BlockSpec((rows, columns), lambda k, order: (order[k], 0))

    def chosen_state(*shape):
        return pl.BlockSpec((1, *shape), lambda k, order: (order[k],) + (0,) * len(shape))

    model_width = output_matrix.shape[2]
    return pl.pallas_call(
        functools.partial(projected_kernel, heads, sizes, len(priors), blocks),
        grid_spec=pltpu.PrefetchScalarGridSpec(
            num_scalar_prefetch=1,
            grid=(blocks,),
            in_specs=[whole(packed_rows, lanes) for _ in priors]
            + [
                chosen(BLOCK, 2 * lanes),
                chosen(BLOCK, width),
                chosen(BLOCK, BLOCK),
                chosen_state(sizes[0], lanes),
                chosen_state(sizes[1], lanes),
                chosen(8, 2 * lanes),
                chosen(BLOCK, 2 * lanes),
                whole(1, 2 * lanes),
                whole(2 * lanes, model_width),
            ],
            out_specs=[whole(BLOCK, model_width)] * blocks,
            scratch_shapes=scratch_shapes,
        ),
        out_shape=[jax.ShapeDtypeStruct((BLOCK, model_width), bf16)] * blocks,
        name="projected",
    )(order, *operands, output_matrix.reshape(2 * lanes, model_width))


def routed_experts(
    wide_stream, normed, gate_weight, up_weight, down_weight, token_expert_choice, expert_output_weight
):
    rows_here, model_width = normed.shape
    expert_total = lax.axis_size("sp")
    capacity = 2 * rows_here // expert_total + 1
    flat_ids = token_expert_choice.reshape(-1)
    matches = (flat_ids[:, None] == jnp.arange(expert_total, dtype=jnp.int32)[None, :]).astype(
        jnp.int32
    )
    slot_rank = jnp.sum((jnp.cumsum(matches, axis=0) - matches) * matches, axis=1)
    target = flat_ids * capacity + slot_rank
    outbound = (
        jnp.zeros((expert_total * capacity, model_width), jnp.bfloat16)
        .at[target]
        .set(jnp.repeat(normed, 2, axis=0))
    )
    outbound = outbound.reshape(expert_total, capacity, model_width)
    widened = lax.all_gather(
        lax.all_to_all(outbound, "sp", split_axis=0, concat_axis=0, tiled=True),
        "tp",
        axis=0,
        tiled=True,
    )
    flat_rows = widened.reshape(-1, widened.shape[-1])
    gate_out = jnp.dot(flat_rows, gate_weight, preferred_element_type=jnp.float32)
    up_out = jnp.dot(flat_rows, up_weight, preferred_element_type=jnp.float32)
    hidden = (jax.nn.silu(gate_out) * up_out).astype(jnp.bfloat16)
    partial_value = jnp.dot(
        hidden, down_weight, preferred_element_type=jnp.float32
    ).astype(jnp.bfloat16)
    partial_value = lax.optimization_barrier(
        partial_value.reshape(widened.shape[0], widened.shape[1], partial_value.shape[-1])
    ).astype(jnp.float32)
    summed = lax.psum_scatter(
        partial_value.astype(jnp.bfloat16), "tp", scatter_dimension=0, tiled=True
    )
    returned = lax.all_to_all(summed, "sp", split_axis=0, concat_axis=0, tiled=True)
    picked = jnp.take(returned.reshape(expert_total * capacity, model_width), target, axis=0)
    picked = picked.reshape(rows_here, 2, model_width).astype(jnp.float32)
    weighted = (
        expert_output_weight[:, 0:1] * picked[:, 0] + expert_output_weight[:, 1:2] * picked[:, 1]
    )
    return (wide_stream + weighted).astype(jnp.bfloat16)


def swapped(array, bit):
    return lax.ppermute(array, "sp", [(i, i ^ bit) for i in range(lax.axis_size("sp"))])


def expert_kernel(region, own_ref, *refs):
    blocks = refs[:4]
    keep_ref, send_ref = refs[7:9]
    gate_ref, up_ref, back_ref, arrived = refs[9:]
    fetches = [
        pltpu.make_async_copy(source, target, arrived.at[i])
        for i, (source, target) in enumerate(zip(refs[4:7], (gate_ref, up_ref, back_ref)))
    ]
    for fetch in fetches:
        fetch.start()
    width = gate_ref.shape[0]
    rows = blocks[0].shape[0]
    own = own_ref[0].astype(jnp.float32)
    place = lax.broadcasted_iota(jnp.int32, (region, rows), 0).astype(jnp.float32)
    before = (
        lax.broadcasted_iota(jnp.int32, (rows, rows), 0)
        < lax.broadcasted_iota(jnp.int32, (rows, rows), 1)
    ).astype(jnp.float32)
    named, weights = [], []
    for block in blocks:
        facts = block[:, width:].astype(jnp.float32).T
        hits = (facts[0:2] == own).astype(jnp.float32)
        named.append(hits[0:1] + hits[1:2])
        weights.append(
            hits[0:1] * (facts[2:3] + facts[4:5]) + hits[1:2] * (facts[3:4] + facts[5:6])
        )
    named = jnp.concatenate(named + [jnp.zeros((4, rows), jnp.float32)], axis=0)
    inner = jnp.dot(named, before, preferred_element_type=jnp.float32)
    slot = jnp.where(named > 0, inner, -1.0)
    taken = []
    for i, block in enumerate(blocks):
        chosen = (place == slot[i : i + 1]).astype(jnp.bfloat16)
        taken.append(jnp.dot(chosen, block[:, :width], preferred_element_type=jnp.float32))
    taken = jnp.concatenate(taken, axis=0).astype(jnp.bfloat16)
    down = jnp.concatenate(
        [slot[0:4]] + weights + [jnp.zeros((rows - 8, rows), jnp.float32)], axis=0
    ).T
    fetches[0].wait()
    gate = jnp.dot(taken, gate_ref[...], preferred_element_type=jnp.float32)
    fetches[1].wait()
    up = jnp.dot(taken, up_ref[...], preferred_element_type=jnp.float32)
    hidden = (gate * jax.nn.sigmoid(gate) * up).astype(jnp.bfloat16)
    fetches[2].wait()
    result = jnp.dot(hidden, back_ref[...], preferred_element_type=jnp.float32)
    place = lax.broadcasted_iota(jnp.int32, (rows, region), 1).astype(jnp.float32)
    for i in range(4):
        chosen = (place == down[:, i : i + 1]).astype(jnp.bfloat16)
        spread = jnp.dot(
            chosen,
            result[i * region : (i + 1) * region].astype(jnp.bfloat16),
            preferred_element_type=jnp.float32,
        )
        out_ref = (keep_ref, send_ref)[i // 2]
        out_ref[i % 2 * rows : (i % 2 + 1) * rows] = (spread * down[:, 4 + i : 5 + i]).astype(
            jnp.bfloat16
        )


def run_expert(blocks, own, gate_weight, up_weight, down_weight, capacity):
    rows = blocks[0].shape[0]
    width, hidden = gate_weight.shape
    region = -(-capacity // 8) * 8
    vmem = pl.BlockSpec(memory_space=pltpu.VMEM)
    return pl.pallas_call(
        functools.partial(expert_kernel, region),
        in_specs=[pl.BlockSpec(memory_space=pltpu.SMEM)] + [vmem] * 4 + [pl.BlockSpec(memory_space=pl.ANY)] * 3,
        out_specs=[vmem] * 2,
        out_shape=[jax.ShapeDtypeStruct((2 * rows, width), jnp.bfloat16)] * 2,
        scratch_shapes=[
            pltpu.VMEM((width, hidden), jnp.bfloat16),
            pltpu.VMEM((width, hidden), jnp.bfloat16),
            pltpu.VMEM((hidden, width), jnp.bfloat16),
            pltpu.SemaphoreType.DMA((3,)),
        ],
        cost_estimate=pl.CostEstimate(
            flops=24 * region * width * hidden,
            bytes_accessed=6 * width * hidden,
            transcendentals=4 * region * hidden,
        ),
        name="expert",
    )(own[None], *blocks, gate_weight, up_weight, down_weight)


def added(block, *received):
    total = block.astype(jnp.float32)
    for other in received:
        if other is not None:
            total = total + other.astype(jnp.float32)
    return total.astype(jnp.bfloat16)


def stream_kernel(
    residual_ref, own_ref, one_ref, two_ref, three_ref, gain_ref, facts_ref, stream_ref, rows_ref
):
    total = own_ref[...].astype(jnp.float32) + residual_ref[...].astype(jnp.float32)
    for ref in (one_ref, two_ref, three_ref):
        total = total + ref[...].astype(jnp.float32)
    stream = total.astype(jnp.bfloat16)
    stream_ref[...] = stream
    wide = stream.astype(jnp.float32)
    scale = lax.rsqrt(jnp.mean(wide * wide, axis=1, keepdims=True) + EPSILON)
    width = wide.shape[1]
    rows_ref[:, :width] = (wide * scale * gain_ref[...]).astype(jnp.bfloat16)
    rows_ref[:, width:] = facts_ref[...]


def stream_and_rows(residual, parts, gain, token_expert_choice, expert_output_weight):
    rows, width = residual.shape
    high = expert_output_weight.astype(jnp.bfloat16)
    low = (expert_output_weight - high.astype(jnp.float32)).astype(jnp.bfloat16)
    facts = jnp.concatenate([token_expert_choice.astype(jnp.bfloat16), high, low], axis=1)
    facts = jnp.pad(facts, ((0, 0), (0, rows - facts.shape[1])))
    return pl.pallas_call(
        stream_kernel,
        out_shape=[
            jax.ShapeDtypeStruct((rows, width), jnp.bfloat16),
            jax.ShapeDtypeStruct((rows, width + rows), jnp.bfloat16),
        ],
        name="stream",
    )(residual, *parts, gain[None], facts)


SWAPS = [(0, 1), (1, 0), (2, 3), (3, 2)]
MIDDLE = [(1, 2), (2, 1)]
ENDS = [(0, 3), (3, 0)]
OUTWARD = [(1, 0), (2, 3)]
INWARD = [(0, 1), (3, 2)]
ARRIVALS = [[0, 1, 3, 2], [1, 0, 2, 3], [2, 3, 1, 0], [3, 2, 0, 1]]


def line_sum(parts):
    ends = lax.ppermute(parts[2], "tp", ENDS)
    middle = lax.ppermute(parts[3], "tp", MIDDLE)
    inward = lax.ppermute(parts[3], "tp", INWARD)
    pair = lax.ppermute(added(parts[1], middle), "tp", SWAPS)
    middle_two = lax.ppermute(added(parts[2], inward), "tp", MIDDLE)
    return parts[0], ends, pair, middle_two


def final_kernel(stream_ref, *refs):
    out_ref = refs[-1]
    total = stream_ref[...].astype(jnp.float32)
    for ref in refs[:-1]:
        total = total + ref[...].astype(jnp.float32)
    out_ref[...] = total.astype(jnp.bfloat16)


def near_kernel_sum(keep_ref, back_ref, out_ref):
    total = keep_ref[...].astype(jnp.float32) + back_ref[...].astype(jnp.float32)
    out_ref[...] = total.astype(jnp.bfloat16)


def near_added(keep, back):
    rows, width = keep.shape
    half = pl.BlockSpec((rows // 2, width), lambda k: (0, 0))
    return pl.pallas_call(
        near_kernel_sum,
        grid=(1,),
        in_specs=[half, half],
        out_specs=half,
        out_shape=jax.ShapeDtypeStruct((rows // 2, width), jnp.bfloat16),
        name="near_sum",
    )(keep, back)


def dense_experts(stream, normed, gate_weight, up_weight, down_weight):
    rows = normed.shape[0]
    capacity = 2 * rows // lax.axis_size("sp") + 1
    place = lax.axis_index("tp")
    mine = lax.axis_index("sp").astype(jnp.int32)
    inner = (place == 1) | (place == 2)

    far = [swapped(normed, 2)]
    from_pair = lax.ppermute(normed, "tp", SWAPS)
    second = lax.ppermute(normed, "tp", MIDDLE + ENDS)
    middle_two = lax.ppermute(from_pair, "tp", MIDDLE)
    outer_two = lax.ppermute(second, "tp", OUTWARD)
    third = jnp.where(inner, middle_two, outer_two)
    blocks = [normed, from_pair, second, third]
    sums = []
    near_other, far_other = [], []
    for turn in range(4):
        if turn:
            far.append(swapped(blocks[turn], 2))
        near_other.append(swapped(blocks[turn], 1))
        far_other.append(swapped(far[turn], 1))
    near_sums, far_sums = [], []
    for turn in range(4):
        keep, send = run_expert(
            [blocks[turn], far[turn], near_other[turn], far_other[turn]],
            mine,
            gate_weight,
            up_weight,
            down_weight,
            capacity,
        )
        back = swapped(send, 1)
        near_sums.append((keep[:rows], back[:rows]))
        if turn == 3:
            near_last = near_added(keep, back)
        far_sums.append(added(keep[rows:], back[rows:]))
    crossed = [swapped(far_sums[turn], 2) for turn in range(4)]
    parts = [None, added(*near_sums[1], crossed[1])]
    parts.append(lax.optimization_barrier(added(*near_sums[2], crossed[2])))
    parts.append(lax.optimization_barrier(added(near_last, crossed[3])))
    sums = line_sum(parts)[1:]
    return pl.pallas_call(
        final_kernel,
        out_shape=jax.ShapeDtypeStruct(stream.shape, jnp.bfloat16),
        name="final",
    )(stream, *near_sums[0], crossed[0], *sums)


def local(
    residual,
    grouped_value_heads,
    output_gate_heads,
    projected_key_query,
    raw_step_size,
    step_size_bias,
    head_decay_logarithm,
    position_extra_decay,
    head_skip_weight,
    value_kernel_taps,
    key_query_kernel,
    head_norm_gain,
    output_matrix,
    expert_norm_gain,
    expert_gate_weight,
    expert_up_weight,
    expert_down_weight,
    token_expert_choice,
    expert_output_weight,
):
    lane_width = grouped_value_heads.shape[2]
    dense = lax.axis_size("sp") == 4 and lax.axis_size("tp") == 4
    order = jnp.asarray(ARRIVALS, jnp.int32)[lax.axis_index("tp")] if dense else None
    mixed_heads = mixed_rows(
        grouped_value_heads,
        output_gate_heads,
        projected_key_query,
        raw_step_size,
        step_size_bias,
        head_decay_logarithm,
        position_extra_decay,
        head_skip_weight,
        value_kernel_taps,
        key_query_kernel,
        head_norm_gain,
        output_matrix,
        order,
    )
    weights = (expert_gate_weight[0], expert_up_weight[0], expert_down_weight[0])
    if dense:
        stream, normed = stream_and_rows(
            residual,
            line_sum(mixed_heads),
            expert_norm_gain,
            token_expert_choice,
            expert_output_weight,
        )
        return dense_experts(stream, normed, *weights)
    model_width = output_matrix.shape[2]
    mix_out = lax.psum_scatter(
        jnp.dot(
            mixed_heads,
            output_matrix.reshape(2 * lane_width, model_width),
            preferred_element_type=jnp.float32,
        ).astype(jnp.bfloat16),
        "tp",
        scatter_dimension=0,
        tiled=True,
    ).astype(jnp.float32)
    stream = (residual.astype(jnp.float32) + mix_out).astype(jnp.bfloat16)
    wide_stream = stream.astype(jnp.float32)
    normed = (
        wide_stream
        * lax.rsqrt(jnp.mean(wide_stream * wide_stream, axis=1, keepdims=True) + EPSILON)
        * expert_norm_gain[None]
    ).astype(jnp.bfloat16)
    return routed_experts(wide_stream, normed, *weights, token_expert_choice, expert_output_weight)


def solution(mesh):
    placed = (
        P(("grp", "sp", "tp"), None),
        P(("grp", "sp"), None, "tp"),
        P(("grp", "sp"), None, "tp"),
        P(("grp", "sp"), None),
        P(("grp", "sp"), None, "tp"),
        P(None, "tp"),
        P(None, "tp"),
        P(("grp", "sp")),
        P(None, "tp"),
        P(None, None, "tp"),
        P(),
        P(None, "tp"),
        P(None, "tp", None),
        P(),
        P("sp", None, "tp"),
        P("sp", None, "tp"),
        P("sp", "tp", None),
        P(("grp", "sp", "tp"), None),
        P(("grp", "sp", "tp"), None),
    )

    return jax.shard_map(
        local, mesh=mesh, in_specs=placed, out_specs=P(("grp", "sp", "tp"), None), check_vma=False
    )
```

profile of v0, /device:TPU:0, one launch (start us, length us, event | category | flops | bytes accessed | tf_op | source)
XLA Modules:
  0.0 283.8 jit_solution(5648235715736802875)
XLA Ops:
  15.0 6.3 %states.1 = (bf16[512,512]{1,0:T(8,128)(2,1)}, bf16[512,384]{1,0:T(8,128)(2,1)}, f32[16,512]{1,0:T(8,128)}, f32[512,128]{1,0:T(8,128)}, f32[4,64,256]{2,1,0:T(8,...) custom-call(bf16[512,512]{1,0:T(8,128)(2,1)} %bitcast.36, bf16[512,384]{1,0:T(8,128)(2,1)} %keys_ref.1, ...), custom_call_target="tpu_custom_call" | custom-call | tf_op jit(solution)/shard_map/states/pallas_call | solution.py:307
  21.3 4.5 %collective-permute-start.1 = (bf16[208,256]{1,0:T(8,128)(2,1)}, bf16[208,256]{1,0:T(8,128)(2,1)S(1)}, u32[]{:S(2)}, u32[]{:S(2)}) collective-permute-start(bf16[208,256]{1,0:T(8,128)(2,1)} %get-tuple-element.27), channel_id=1, source_target_pairs={{0,4},{4,8},{8,12},{1,5},{5,9},{9,13},{2,6},{6,10},{10,14},{3,7},{... | collective-permute-start | bytes 319496 | tf_op jit(solution)/shard_map/ppermute | solution.py:23
  30.3 4.6 %near.1.refs_3_ = f32[512,512]{1,0:T(8,128)} custom-call(bf16[512,512]{1,0:T(8,128)(2,1)} %get-tuple-element.28.x_ref, bf16[512,384]{1,0:T(8,128)(2,1)} %get-tuple-element.29.rows_ref.refs_4_, f32[16,512]{1,0:T(8,128)} %get-tuple-element.30.across_ref, f32[512,128]{1,0:T(8,128)} %get-tuple-element.31.down_ref.refs_5_, f32[8,3]{1,0:T(8,128)} %pad_maximum_fusion.1.facts_ref), custom_call_target="tpu_custom_call" | custom-call | tf_op jit(solution)/shard_map/near/pallas_call | solution.py:358
  35.7 11.3 %projected.1 = (bf16[128,2048]{1,0:T(8,128)(2,1)}, bf16[128,2048]{1,0:T(8,128)(2,1)}, bf16[128,2048]{1,0:T(8,128)(2,1)}, bf16[128,2048]{1,0:T(8,128)(2,1)}) custom-call(s32[4]{0:T(128)} %dynamic-slice_bitcast_fusion.order_ref, bf16[208,256]{1,0:T(8,128)(2,1)} %copy-done.16, bf16[208,256]{1,0:T(8,128)(2,1)} %copy-done.17, bf16[208,256]{1,0:T(8,128)(2,1)} %copy-done.18, ...), custom_call_target="tpu_custom_call" | custom-call | tf_op jit(solution)/shard_map/projected/pallas_call | solution.py:415
  46.9 3.5 %collective-permute-start.7 = (bf16[128,2048]{1,0:T(8,128)(2,1)}, bf16[128,2048]{1,0:T(8,128)(2,1)S(1)}, u32[]{:S(2)}, u32[]{:S(2)}) collective-permute-start(bf16[128,2048]{1,0:T(8,128)(2,1)} %get-tuple-element.38), channel_id=1, source_target_pairs={{0,1},{3,2},{4,5},{7,6},{8,9},{11,10},{12,13},{15,14},{16,17},{19,... | collective-permute-start | bytes 1572872 | tf_op jit(solution)/shard_map/ppermute | solution.py:623
  51.2 4.4 %collective-permute-start.4 = (bf16[128,2048]{1,0:T(8,128)(2,1)}, bf16[128,2048]{1,0:T(8,128)(2,1)S(1)}, u32[]{:S(2)}, u32[]{:S(2)}) collective-permute-start(bf16[128,2048]{1,0:T(8,128)(2,1)} %get-tuple-element.36), channel_id=1, source_target_pairs={{0,3},{3,0},{4,7},{7,4},{8,11},{11,8},{12,15},{15,12},{16,19},{19,... | collective-permute-start | bytes 1572872 | tf_op jit(solution)/shard_map/ppermute | solution.py:621
  55.5 7.5 %collective-permute-done.7 = bf16[128,2048]{1,0:T(8,128)(2,1)S(1)} collective-permute-done((bf16[128,2048]{1,0:T(8,128)(2,1)}, bf16[128,2048]{1,0:T(8,128)(2,1)S(1)}, u32[]{:S(2)}, u32[]{:S(2)}) %collective-permute-start.7) | collective-permute-done | bytes 524320 | tf_op jit(solution)/shard_map/ppermute | solution.py:623
  66.1 11.3 %collective-permute-start.6 = (bf16[128,2048]{1,0:T(8,128)(2,1)S(1)}, bf16[128,2048]{1,0:T(8,128)(2,1)S(1)}, u32[]{:S(2)}, u32[]{:S(2)}) collective-permute-start(bf16[128,2048]{1,0:T(8,128)(2,1)S(1)} %add_convert_fusion.10), channel_id=1, source_target_pairs={{0,1},{1,0},{2,3},{3,2},{4,5},{5,4},{6,7},{7,6},{8,9},{9,8},{10,11... | collective-permute-start | bytes 1572872 | tf_op jit(solution)/shard_map/ppermute | solution.py:624
  78.3 8.1 %collective-permute-done.6.two_ref = bf16[128,2048]{1,0:T(8,128)(2,1)S(1)} collective-permute-done((bf16[128,2048]{1,0:T(8,128)(2,1)S(1)}, bf16[128,2048]{1,0:T(8,128)(2,1)S(1)}, u32[]{:S(2)}, u32[]{:S(2)}) %collective-permute-start.6) | collective-permute-done | bytes 524320 | tf_op jit(solution)/shard_map/ppermute | solution.py:624
  93.9 11.5 %collective-permute-done.21.refs_0_ = bf16[128,2176]{1,0:T(8,128)(2,1)S(1)} collective-permute-done((bf16[128,2176]{1,0:T(8,128)(2,1)}, bf16[128,2176]{1,0:T(8,128)(2,1)S(1)}, u32[]{:S(2)}, u32[]{:S(2)}) %collective-permute-start.21) | collective-permute-done | bytes 557088 | tf_op jit(solution)/shard_map/ppermute | solution.py:663
  106.1 11.0 %collective-permute-done.14.refs_0_ = bf16[128,2176]{1,0:T(8,128)(2,1)S(1)} collective-permute-done((bf16[128,2176]{1,0:T(8,128)(2,1)}, bf16[128,2176]{1,0:T(8,128)(2,1)S(1)}, u32[]{:S(2)}, u32[]{:S(2)}) %collective-permute-start.14) | collective-permute-done | bytes 557088 | tf_op jit(solution)/shard_map/ppermute | solution.py:664
  118.6 12.5 %collective-permute-done.28 = bf16[128,2176]{1,0:T(8,128)(2,1)S(1)} collective-permute-done((bf16[128,2176]{1,0:T(8,128)(2,1)S(1)}, bf16[128,2176]{1,0:T(8,128)(2,1)S(1)}, u32[]{:S(2)}, u32[]{:S(2)}) %collective-permute-start.28) | collective-permute-done | bytes 557088 | tf_op jit(solution)/shard_map/ppermute | solution.py:666
  133.4 13.5 %collective-permute-done.29.refs_1_ = bf16[128,2176]{1,0:T(8,128)(2,1)} collective-permute-done((bf16[128,2176]{1,0:T(8,128)(2,1)S(1)}, bf16[128,2176]{1,0:T(8,128)(2,1)}, u32[]{:S(2)}, u32[]{:S(2)}) %collective-permute-start.29) | collective-permute-done | bytes 557088 | tf_op jit(solution)/shard_map/ppermute | solution.py:487
  147.4 11.3 %collective-permute-done.9.refs_1_ = bf16[128,2176]{1,0:T(8,128)(2,1)S(1)} collective-permute-done((bf16[128,2176]{1,0:T(8,128)(2,1)}, bf16[128,2176]{1,0:T(8,128)(2,1)S(1)}, u32[]{:S(2)}, u32[]{:S(2)}) %collective-permute-start.9) | collective-permute-done | bytes 557088 | tf_op jit(solution)/shard_map/ppermute | solution.py:487
  158.7 11.9 %collective-permute-done.15.refs_1_ = bf16[128,2176]{1,0:T(8,128)(2,1)S(1)} collective-permute-done((bf16[128,2176]{1,0:T(8,128)(2,1)S(1)}, bf16[128,2176]{1,0:T(8,128)(2,1)S(1)}, u32[]{:S(2)}, u32[]{:S(2)}) %collective-permute-start.15) | collective-permute-done | bytes 557088 | tf_op jit(solution)/shard_map/ppermute | solution.py:487
  171.3 9.6 %expert.7 = (bf16[256,2048]{1,0:T(8,128)(2,1)}, bf16[256,2048]{1,0:T(8,128)(2,1)}) custom-call(s32[1]{0:T(128)} %bitcast.5.own_ref, bf16[128,2176]{1,0:T(8,128)(2,1)} %copy-done.2, bf16[128,2176]{1,0:T(8,128)(2,1)} %collective-permute-done.29.refs_1_, bf16[128,2176]{1,0:T(8,128)(2,1)} %collective-permute-done.30.refs_2_, ...), custom_call_target="tpu_custom_call" | custom-call | flops 3623878656 | bytes 12582912 | tf_op jit(solution)/shard_map/expert/pallas_call | solution.py:553
  181.9 9.6 %expert.4 = (bf16[256,2048]{1,0:T(8,128)(2,1)}, bf16[256,2048]{1,0:T(8,128)(2,1)}) custom-call(s32[1]{0:T(128)} %bitcast.5.own_ref, bf16[128,2176]{1,0:T(8,128)(2,1)} %get-tuple-element.40.refs_0_, bf16[128,2176]{1,0:T(8,128)(2,1)} %copy-done.9, bf16[128,2176]{1,0:T(8,128)(2,1)} %collective-permute-done.10.refs_2_, ...), custom_call_target="tpu_custom_call" | custom-call | flops 3623878656 | bytes 12582912 | tf_op jit(solution)/shard_map/expert/pallas_call | solution.py:553
  191.6 9.8 %expert.5 = (bf16[256,2048]{1,0:T(8,128)(2,1)}, bf16[256,2048]{1,0:T(8,128)(2,1)}) custom-call(s32[1]{0:T(128)} %bitcast.5.own_ref, bf16[128,2176]{1,0:T(8,128)(2,1)} %copy-done.7, bf16[128,2176]{1,0:T(8,128)(2,1)} %copy-done.8, bf16[128,2176]{1,0:T(8,128)(2,1)} %collective-permute-done.16.refs_2_, bf16[128,2176]{1,0:T(8,128)(2,1)} %collective-permute-done.17.refs_3_, ...), custom_call_target="tpu_custom_call" | custom-call | flops 3623878656 | bytes 12582912 | tf_op jit(solution)/shard_map/expert/pallas_call | solution.py:553
  201.9 9.6 %expert.6 = (bf16[256,2048]{1,0:T(8,128)(2,1)}, bf16[256,2048]{1,0:T(8,128)(2,1)}) custom-call(s32[1]{0:T(128)} %bitcast.5.own_ref, bf16[128,2176]{1,0:T(8,128)(2,1)} %copy-done.6, bf16[128,2176]{1,0:T(8,128)(2,1)} %collective-permute-done.22.refs_1_, bf16[128,2176]{1,0:T(8,128)(2,1)} %collective-permute-done.23.refs_2_, ...), custom_call_target="tpu_custom_call" | custom-call | flops 3623878656 | bytes 12582912 | tf_op jit(solution)/shard_map/expert/pallas_call | solution.py:553
  221.2 6.6 %collective-permute-done.33 = bf16[128,2048]{1,0:T(8,128)(2,1)} collective-permute-done((bf16[128,2048]{1,0:T(8,128)(2,1)}, bf16[128,2048]{1,0:T(8,128)(2,1)}, u32[]{:S(2)}, u32[]{:S(2)}) %collective-permute-start.33) | collective-permute-done | bytes 524320 | tf_op jit(solution)/shard_map/ppermute | solution.py:487
  232.7 17.5 %collective-permute-done.19 = bf16[128,2048]{1,0:T(8,128)(2,1)} collective-permute-done((bf16[128,2048]{1,0:T(8,128)(2,1)}, bf16[128,2048]{1,0:T(8,128)(2,1)}, u32[]{:S(2)}, u32[]{:S(2)}) %collective-permute-start.19) | collective-permute-done | bytes 524320 | tf_op jit(solution)/shard_map/ppermute | solution.py:487
  251.7 5.8 %collective-permute-start.20 = (bf16[128,2048]{1,0:T(8,128)(2,1)S(1)}, bf16[128,2048]{1,0:T(8,128)(2,1)S(1)}, u32[]{:S(2)}, u32[]{:S(2)}) collective-permute-start(bf16[128,2048]{1,0:T(8,128)(2,1)S(1)} %add_convert_fusion.6), channel_id=1, source_target_pairs={{0,3},{3,0},{4,7},{7,4},{8,11},{11,8},{12,15},{15,12},{16,19},{19,... | collective-permute-start | bytes 1572872 | tf_op jit(solution)/shard_map/ppermute | solution.py:621
  265.0 5.3 %collective-permute-done.20.refs_3_ = bf16[128,2048]{1,0:T(8,128)(2,1)S(1)} collective-permute-done((bf16[128,2048]{1,0:T(8,128)(2,1)S(1)}, bf16[128,2048]{1,0:T(8,128)(2,1)S(1)}, u32[]{:S(2)}, u32[]{:S(2)}) %collective-permute-start.20) | collective-permute-done | bytes 524320 | tf_op jit(solution)/shard_map/ppermute | solution.py:621
  270.3 9.5 %collective-permute-done.35.refs_4_ = bf16[128,2048]{1,0:T(8,128)(2,1)S(1)} collective-permute-done((bf16[128,2048]{1,0:T(8,128)(2,1)S(1)}, bf16[128,2048]{1,0:T(8,128)(2,1)S(1)}, u32[]{:S(2)}, u32[]{:S(2)}) %collective-permute-start.35) | collective-permute-done | bytes 524320 | tf_op jit(solution)/shard_map/ppermute | solution.py:624
  (138 shorter events, 66.8 us)
Async XLA Ops:
  46.9 16.1 %collective-permute-start.7 = (bf16[128,2048]{1,0:T(8,128)(2,1)}, bf16[128,2048]{1,0:T(8,128)(2,1)S(1)}, u32[]{:S(2)}, u32[]{:S(2)}) collective-permute-start(bf16[128,2048]{1,0:T(8,128)(2,1)} %get-tuple-element.38), channel_id=1, source_target_pairs={{0,1},{3,2},{4,5},{7,6},{8,9},{11,10},{12,13},{15,14},{16,17},{19,... | collective-permute-start | bytes 1572872 | tf_op jit(solution)/shard_map/ppermute | solution.py:623
  51.2 27.1 %collective-permute-start.4 = (bf16[128,2048]{1,0:T(8,128)(2,1)}, bf16[128,2048]{1,0:T(8,128)(2,1)S(1)}, u32[]{:S(2)}, u32[]{:S(2)}) collective-permute-start(bf16[128,2048]{1,0:T(8,128)(2,1)} %get-tuple-element.36), channel_id=1, source_target_pairs={{0,3},{3,0},{4,7},{7,4},{8,11},{11,8},{12,15},{15,12},{16,19},{19,... | collective-permute-start | bytes 1572872 | tf_op jit(solution)/shard_map/ppermute | solution.py:621
  66.1 20.2 %collective-permute-start.6 = (bf16[128,2048]{1,0:T(8,128)(2,1)S(1)}, bf16[128,2048]{1,0:T(8,128)(2,1)S(1)}, u32[]{:S(2)}, u32[]{:S(2)}) collective-permute-start(bf16[128,2048]{1,0:T(8,128)(2,1)S(1)} %add_convert_fusion.10), channel_id=1, source_target_pairs={{0,1},{1,0},{2,3},{3,2},{4,5},{5,4},{6,7},{7,6},{8,9},{9,8},{10,11... | collective-permute-start | bytes 1572872 | tf_op jit(solution)/shard_map/ppermute | solution.py:624
  91.1 26.0 %collective-permute-start.14 = (bf16[128,2176]{1,0:T(8,128)(2,1)}, bf16[128,2176]{1,0:T(8,128)(2,1)S(1)}, u32[]{:S(2)}, u32[]{:S(2)}) collective-permute-start(bf16[128,2176]{1,0:T(8,128)(2,1)} %get-tuple-element.40.refs_0_), channel_id=1, source_target_pairs={{1,2},{2,1},{0,3},{3,0},{5,6},{6,5},{4,7},{7,4},{9,10},{10,9},{8,1... | collective-permute-start | bytes 1671176 | tf_op jit(solution)/shard_map/ppermute | solution.py:664
  131.3 27.4 %collective-permute-start.9 = (bf16[128,2176]{1,0:T(8,128)(2,1)}, bf16[128,2176]{1,0:T(8,128)(2,1)S(1)}, u32[]{:S(2)}, u32[]{:S(2)}) collective-permute-start(bf16[128,2176]{1,0:T(8,128)(2,1)} %get-tuple-element.40.refs_0_), channel_id=1, source_target_pairs={{0,8},{4,12},{8,0},{12,4},{1,9},{5,13},{9,1},{13,5},{2,10},{6,14},... | collective-permute-start | bytes 1671176 | tf_op jit(solution)/shard_map/ppermute | solution.py:487
  133.3 37.3 %collective-permute-start.15 = (bf16[128,2176]{1,0:T(8,128)(2,1)S(1)}, bf16[128,2176]{1,0:T(8,128)(2,1)S(1)}, u32[]{:S(2)}, u32[]{:S(2)}) collective-permute-start(bf16[128,2176]{1,0:T(8,128)(2,1)S(1)} %collective-permute-done.14.refs_0_), channel_id=1, source_target_pairs={{0,8},{4,12},{8,0},{12,4},{1,9},{5,13},{9,1},{13,5},{2,10},{6,14},... | collective-permute-start | bytes 1671176 | tf_op jit(solution)/shard_map/ppermute | solution.py:487
  133.4 37.3 %collective-permute-start.30 = (bf16[128,2176]{1,0:T(8,128)(2,1)S(1)}, bf16[128,2176]{1,0:T(8,128)(2,1)}, u32[]{:S(2)}, u32[]{:S(2)}) collective-permute-start(bf16[128,2176]{1,0:T(8,128)(2,1)S(1)} %broadcast_select_fusion.refs_0_), channel_id=1, source_target_pairs={{0,4},{4,0},{8,12},{12,8},{1,5},{5,1},{9,13},{13,9},{2,6},{6,2},{1... | collective-permute-start | bytes 1671176 | tf_op jit(solution)/shard_map/ppermute | solution.py:487
  146.9 24.3 %collective-permute-start.31 = (bf16[128,2176]{1,0:T(8,128)(2,1)}, bf16[128,2176]{1,0:T(8,128)(2,1)}, u32[]{:S(2)}, u32[]{:S(2)}) collective-permute-start(bf16[128,2176]{1,0:T(8,128)(2,1)} %collective-permute-done.29.refs_1_), channel_id=1, source_target_pairs={{0,4},{4,0},{8,12},{12,8},{1,5},{5,1},{9,13},{13,9},{2,6},{6,2},{1... | collective-permute-start | bytes 1671176 | tf_op jit(solution)/shard_map/ppermute | solution.py:487
  146.9 34.0 %collective-permute-start.10 = (bf16[128,2176]{1,0:T(8,128)(2,1)}, bf16[128,2176]{1,0:T(8,128)(2,1)}, u32[]{:S(2)}, u32[]{:S(2)}) collective-permute-start(bf16[128,2176]{1,0:T(8,128)(2,1)} %get-tuple-element.40.refs_0_), channel_id=1, source_target_pairs={{0,4},{4,0},{8,12},{12,8},{1,5},{5,1},{9,13},{13,9},{2,6},{6,2},{1... | collective-permute-start | bytes 1671176 | tf_op jit(solution)/shard_map/ppermute | solution.py:487
  158.7 22.6 %collective-permute-start.22 = (bf16[128,2176]{1,0:T(8,128)(2,1)S(1)}, bf16[128,2176]{1,0:T(8,128)(2,1)}, u32[]{:S(2)}, u32[]{:S(2)}) collective-permute-start(bf16[128,2176]{1,0:T(8,128)(2,1)S(1)} %collective-permute-done.21.refs_0_), channel_id=1, source_target_pairs={{0,8},{4,12},{8,0},{12,4},{1,9},{5,13},{9,1},{13,5},{2,10},{6,14},... | collective-permute-start | bytes 1671176 | tf_op jit(solution)/shard_map/ppermute | solution.py:487
  170.7 20.8 %collective-permute-start.16 = (bf16[128,2176]{1,0:T(8,128)(2,1)S(1)}, bf16[128,2176]{1,0:T(8,128)(2,1)}, u32[]{:S(2)}, u32[]{:S(2)}) collective-permute-start(bf16[128,2176]{1,0:T(8,128)(2,1)S(1)} %collective-permute-done.14.refs_0_), channel_id=1, source_target_pairs={{0,4},{4,0},{8,12},{12,8},{1,5},{5,1},{9,13},{13,9},{2,6},{6,2},{1... | collective-permute-start | bytes 1671176 | tf_op jit(solution)/shard_map/ppermute | solution.py:487
  171.2 20.5 %collective-permute-start.17 = (bf16[128,2176]{1,0:T(8,128)(2,1)S(1)}, bf16[128,2176]{1,0:T(8,128)(2,1)}, u32[]{:S(2)}, u32[]{:S(2)}) collective-permute-start(bf16[128,2176]{1,0:T(8,128)(2,1)S(1)} %collective-permute-done.15.refs_1_), channel_id=1, source_target_pairs={{0,4},{4,0},{8,12},{12,8},{1,5},{5,1},{9,13},{13,9},{2,6},{6,2},{1... | collective-permute-start | bytes 1671176 | tf_op jit(solution)/shard_map/ppermute | solution.py:487
  180.9 30.9 %collective-permute-start.32 = (bf16[256,2048]{1,0:T(8,128)(2,1)}, bf16[256,2048]{1,0:T(8,128)(2,1)S(1)}, u32[]{:S(2)}, u32[]{:S(2)}) collective-permute-start(bf16[256,2048]{1,0:T(8,128)(2,1)} %get-tuple-element.48), channel_id=1, source_target_pairs={{0,4},{4,0},{8,12},{12,8},{1,5},{5,1},{9,13},{13,9},{2,6},{6,2},{1... | collective-permute-start | bytes 3145736 | tf_op jit(solution)/shard_map/ppermute | solution.py:487
  181.4 20.5 %collective-permute-start.23 = (bf16[128,2176]{1,0:T(8,128)(2,1)S(1)}, bf16[128,2176]{1,0:T(8,128)(2,1)}, u32[]{:S(2)}, u32[]{:S(2)}) collective-permute-start(bf16[128,2176]{1,0:T(8,128)(2,1)S(1)} %collective-permute-done.21.refs_0_), channel_id=1, source_target_pairs={{0,4},{4,0},{8,12},{12,8},{1,5},{5,1},{9,13},{13,9},{2,6},{6,2},{1... | collective-permute-start | bytes 1671176 | tf_op jit(solution)/shard_map/ppermute | solution.py:487
  181.5 20.4 %collective-permute-start.24 = (bf16[128,2176]{1,0:T(8,128)(2,1)}, bf16[128,2176]{1,0:T(8,128)(2,1)}, u32[]{:S(2)}, u32[]{:S(2)}) collective-permute-start(bf16[128,2176]{1,0:T(8,128)(2,1)} %collective-permute-done.22.refs_1_), channel_id=1, source_target_pairs={{0,4},{4,0},{8,12},{12,8},{1,5},{5,1},{9,13},{13,9},{2,6},{6,2},{1... | collective-permute-start | bytes 1671176 | tf_op jit(solution)/shard_map/ppermute | solution.py:487
  191.5 21.2 %collective-permute-start.12 = (bf16[256,2048]{1,0:T(8,128)(2,1)}, bf16[256,2048]{1,0:T(8,128)(2,1)}, u32[]{:S(2)}, u32[]{:S(2)}) collective-permute-start(bf16[256,2048]{1,0:T(8,128)(2,1)} %get-tuple-element.42), channel_id=1, source_target_pairs={{0,4},{4,0},{8,12},{12,8},{1,5},{5,1},{9,13},{13,9},{2,6},{6,2},{1... | collective-permute-start | bytes 3145736 | tf_op jit(solution)/shard_map/ppermute | solution.py:487
  211.5 19.3 %collective-permute-start.25 = (bf16[256,2048]{1,0:T(8,128)(2,1)}, bf16[256,2048]{1,0:T(8,128)(2,1)}, u32[]{:S(2)}, u32[]{:S(2)}) collective-permute-start(bf16[256,2048]{1,0:T(8,128)(2,1)} %get-tuple-element.46), channel_id=1, source_target_pairs={{0,4},{4,0},{8,12},{12,8},{1,5},{5,1},{9,13},{13,9},{2,6},{6,2},{1... | collective-permute-start | bytes 3145736 | tf_op jit(solution)/shard_map/ppermute | solution.py:487
  214.9 50.0 %collective-permute-start.13 = (bf16[128,2048]{1,0:T(8,128)(2,1)}, bf16[128,2048]{1,0:T(8,128)(2,1)}, u32[]{:S(2)}, u32[]{:S(2)}) collective-permute-start(bf16[128,2048]{1,0:T(8,128)(2,1)} %add_convert_fusion.8), channel_id=1, source_target_pairs={{0,8},{4,12},{8,0},{12,4},{1,9},{5,13},{9,1},{13,5},{2,10},{6,14},... | collective-permute-start | bytes 1572872 | tf_op jit(solution)/shard_map/ppermute | solution.py:487
  219.1 31.2 %collective-permute-start.19 = (bf16[128,2048]{1,0:T(8,128)(2,1)}, bf16[128,2048]{1,0:T(8,128)(2,1)}, u32[]{:S(2)}, u32[]{:S(2)}) collective-permute-start(bf16[128,2048]{1,0:T(8,128)(2,1)} %add_convert_fusion.7), channel_id=1, source_target_pairs={{0,8},{4,12},{8,0},{12,4},{1,9},{5,13},{9,1},{13,5},{2,10},{6,14},... | collective-permute-start | bytes 1572872 | tf_op jit(solution)/shard_map/ppermute | solution.py:487
  229.1 28.4 %collective-permute-start.36 = (bf16[128,2048]{1,0:T(8,128)(2,1)S(1)}, bf16[128,2048]{1,0:T(8,128)(2,1)S(1)}, u32[]{:S(2)}, u32[]{:S(2)}) collective-permute-start(bf16[128,2048]{1,0:T(8,128)(2,1)S(1)} %add_convert_fusion.2), channel_id=1, source_target_pairs={{0,1},{3,2},{4,5},{7,6},{8,9},{11,10},{12,13},{15,14},{16,17},{19,... | collective-permute-start | bytes 1572872 | tf_op jit(solution)/shard_map/ppermute | solution.py:623
  232.0 28.8 %collective-permute-start.26 = (bf16[128,2048]{1,0:T(8,128)(2,1)S(1)}, bf16[128,2048]{1,0:T(8,128)(2,1)S(1)}, u32[]{:S(2)}, u32[]{:S(2)}) collective-permute-start(bf16[128,2048]{1,0:T(8,128)(2,1)S(1)} %add_convert_fusion.5), channel_id=1, source_target_pairs={{0,8},{4,12},{8,0},{12,4},{1,9},{5,13},{9,1},{13,5},{2,10},{6,14},... | collective-permute-start | bytes 1572872 | tf_op jit(solution)/shard_map/ppermute | solution.py:487
  232.0 28.7 %collective-permute-start.34 = (bf16[128,2048]{1,0:T(8,128)(2,1)S(1)}, bf16[128,2048]{1,0:T(8,128)(2,1)S(1)}, u32[]{:S(2)}, u32[]{:S(2)}) collective-permute-start(bf16[128,2048]{1,0:T(8,128)(2,1)S(1)} %add_convert_fusion.2), channel_id=1, source_target_pairs={{1,2},{2,1},{5,6},{6,5},{9,10},{10,9},{13,14},{14,13},{17,18},{18,... | collective-permute-start | bytes 1572872 | tf_op jit(solution)/shard_map/ppermute | solution.py:622
  251.7 18.5 %collective-permute-start.20 = (bf16[128,2048]{1,0:T(8,128)(2,1)S(1)}, bf16[128,2048]{1,0:T(8,128)(2,1)S(1)}, u32[]{:S(2)}, u32[]{:S(2)}) collective-permute-start(bf16[128,2048]{1,0:T(8,128)(2,1)S(1)} %add_convert_fusion.6), channel_id=1, source_target_pairs={{0,3},{3,0},{4,7},{7,4},{8,11},{11,8},{12,15},{15,12},{16,19},{19,... | collective-permute-start | bytes 1572872 | tf_op jit(solution)/shard_map/ppermute | solution.py:621
  262.1 17.6 %collective-permute-start.35 = (bf16[128,2048]{1,0:T(8,128)(2,1)S(1)}, bf16[128,2048]{1,0:T(8,128)(2,1)S(1)}, u32[]{:S(2)}, u32[]{:S(2)}) collective-permute-start(bf16[128,2048]{1,0:T(8,128)(2,1)S(1)} %add_convert_fusion.1), channel_id=1, source_target_pairs={{0,1},{1,0},{2,3},{3,2},{4,5},{5,4},{6,7},{7,6},{8,9},{9,8},{10,11... | collective-permute-start | bytes 1572872 | tf_op jit(solution)/shard_map/ppermute | solution.py:624
  (36 other events, 626.0 us)
where the time goes:
time: 285 us; the launch traced here: 284 us
  waiting for transfers between devices  129 us (45%)
  Pallas kernels  69.1 us (24%)
  starting transfers between devices  52.6 us (18%)
  local copies, waits for them, and re-layouts  19 us (7%)
  other arithmetic  13.8 us (5%)
    ppermute x20, waiting for transfers between devices, swapped(): lax.ppermute(array, 'sp', [(i, i ^ bit) for i in range(lax.axis_size('sp'...  63.3 us
    pallas_call x4, Pallas kernels, run_expert(): pl.pallas_call(functools.partial(expert_kernel, region), in_specs=[pl.Blo...  38.5 us
    ppermute x2, waiting for transfers between devices, line_sum(): pair = lax.ppermute(added(parts[1], middle), 'tp', SWAPS)  17.5 us
    convert_element_type x10, other arithmetic, added(): return total.astype(jnp.bfloat16)  13 us
    ppermute x1, waiting for transfers between devices, dense_experts(): outer_two = lax.ppermute(second, 'tp', OUTWARD)  12.5 us
    ppermute x1, waiting for transfers between devices, dense_experts(): from_pair = lax.ppermute(normed, 'tp', SWAPS)  11.5 us
    ppermute x2, starting transfers between devices, line_sum(): pair = lax.ppermute(added(parts[1], middle), 'tp', SWAPS)  11.4 us
    pallas_call x1, Pallas kernels, mixed_rows(): pl.pallas_call(functools.partial(projected_kernel, heads, sizes, len(prio...  11.3 us
  transfers between devices with their start and end apart: 38, of which 13 were waited for; matrix products, arithmetic and copies ran while one was open for 10% of the time, Pallas kernels for 16%

commit v1 on v0

--- a/solution.py
+++ b/solution.py
@@ -44,6 +44,19 @@
     return jnp.concatenate(
         [spread_down(tall, g * heads, heads, width) for g in range(2)], axis=1
     )
+
+
+def head_facts(facts_ref, kind, high):
+    heads = facts_ref.shape[1]
+    both = jnp.concatenate(
+        [facts_ref[2 * kind : 2 * kind + 1], facts_ref[2 * kind + 1 : 2 * kind + 2]], axis=1
+    )
+    if high > 2 * heads:
+        both = jnp.concatenate([both, jnp.zeros((1, high - 2 * heads), jnp.float32)], axis=1)
+    same = lax.broadcasted_iota(jnp.int32, (high, high), 0) == lax.broadcasted_iota(
+        jnp.int32, (high, high), 1
+    )
+    return jnp.sum(jnp.where(same, jnp.broadcast_to(both, (high, high)), 0.0), axis=1, keepdims=True)
 
 
 def states_kernel(
@@ -82,12 +95,16 @@
         sum_ref[...] = jnp.zeros_like(sum_ref)
 
     here = jnp.concatenate(
-        [values_ref[...].astype(jnp.float32), keys_ref[...].astype(jnp.float32)], axis=1
+        [values_ref[:, g].astype(jnp.float32) for g in range(2)]
+        + [keys_ref[...].astype(jnp.float32)],
+        axis=1,
     )
     extended = jnp.concatenate([tail_ref[...], here], axis=0)
     tail_ref[...] = here[BLOCK - 8 :]
     weights = jnp.concatenate(
-        [value_taps_ref[...].astype(jnp.float32), key_taps_ref[...].astype(jnp.float32)], axis=1
+        [value_taps_ref[:, g].astype(jnp.float32) for g in range(2)]
+        + [key_taps_ref[...].astype(jnp.float32)],
+        axis=1,
     )
     summed = jnp.zeros_like(here)
     for j in range(taps):
@@ -99,9 +116,13 @@
     x_ref[...] = x
     rows_ref[...] = rows
 
-    raw = steps_ref[...] + facts_ref[:, 0:1]
+    high = high_rows(heads)
+    raw = [steps_ref[g].astype(jnp.float32) for g in range(2)]
+    if high > 2 * heads:
+        raw.append(jnp.zeros((high - 2 * heads, BLOCK), jnp.float32))
+    raw = jnp.concatenate(raw, axis=0) + head_facts(facts_ref, 0, high)
     stride = jnp.maximum(raw, 0.0) + jnp.log1p(jnp.exp(-jnp.abs(raw)))
-    log_decay = extra_ref[...] - jnp.exp(facts_ref[:, 1:2]) * stride
+    log_decay = extra_ref[...] - jnp.exp(head_facts(facts_ref, 1, high)) * stride
     upto = (
         lax.broadcasted_iota(jnp.int32, (BLOCK, BLOCK), 0)
         <= lax.broadcasted_iota(jnp.int32, (BLOCK, BLOCK), 1)
@@ -111,7 +132,6 @@
     )
     end = running[:, BLOCK - 1 :]
     fading = jnp.exp(end - running) * stride
-    high = running.shape[0]
     stacked = jnp.concatenate(
         [running, fading, jnp.exp(running)]
         + [jnp.zeros((BLOCK - 3 * high, BLOCK), jnp.float32)],
@@ -161,7 +181,7 @@
     later = lax.broadcasted_iota(jnp.int32, (BLOCK, BLOCK), 0) >= lax.broadcasted_iota(
         jnp.int32, (BLOCK, BLOCK), 1
     )
-    skip = both_groups(facts_ref[:, 2:3], heads, HEAD_DIM)
+    skip = both_groups(head_facts(facts_ref, 2, high), heads, HEAD_DIM)
     bound = 0
     out = []
     for g in range(2):
@@ -223,7 +243,7 @@
             queries, entering.astype(jnp.bfloat16), preferred_element_type=jnp.float32
         )
         reach = down_ref[:, 2 * high + g * heads : 2 * high + (g + 1) * heads]
-        gate = gate_ref[:, here].astype(jnp.float32)
+        gate = gate_ref[:, g].astype(jnp.float32)
         total = near_ref[:, here] + far * widened(reach, heads, HEAD_DIM)
         gated = total * (gate * jax.nn.sigmoid(gate))
         squares = gated * gated
@@ -235,7 +255,7 @@
             axis=1,
         ) * (1.0 / HEAD_DIM)
         scale = widened(lax.rsqrt(means + EPSILON), heads, HEAD_DIM)
-        out.append((gated * scale * gain_ref[:, here]).astype(jnp.bfloat16))
+        out.append((gated * scale * gain_ref[g : g + 1]).astype(jnp.bfloat16))
     return jnp.concatenate(out, axis=1)
 
 
@@ -281,14 +301,8 @@
     rim = passed_along(
         jnp.concatenate([last, projected_key_query[positions - 8 :]], axis=1), "sp", 1
     )
-    values = grouped_value_heads.reshape(positions, 2 * lanes)
-    facts = jnp.stack(
-        [step_size_bias.reshape(-1), head_decay_logarithm.reshape(-1), head_skip_weight.reshape(-1)],
-        axis=1,
-    )
-    facts = jnp.pad(facts, ((0, high - 2 * heads), (0, 0)))
-    steps = raw_step_size.reshape(positions, 2 * heads).T.astype(jnp.float32)
-    steps = jnp.pad(steps, ((0, high - 2 * heads), (0, 0)))
+    facts = jnp.concatenate([step_size_bias, head_decay_logarithm, head_skip_weight], axis=0)
+    steps = raw_step_size.transpose(1, 2, 0)
 
     def by_block(rows, columns):
         return pl.BlockSpec((rows, columns), lambda k: (k, 0))
@@ -308,13 +322,13 @@
         functools.partial(states_kernel, heads, sizes),
         grid=(blocks,),
         in_specs=[
-            by_block(BLOCK, 2 * lanes),
+            pl.BlockSpec((BLOCK, 2, lanes), lambda k: (k, 0, 0)),
             by_block(BLOCK, width),
             fixed(8, 2 * lanes + width),
-            fixed(value_kernel_taps.shape[0], 2 * lanes),
+            fixed(*value_kernel_taps.shape),
             fixed(*key_query_kernel.shape),
-            along(high),
-            fixed(high, 3),
+            pl.BlockSpec((2, heads, BLOCK), lambda k: (0, 0, k)),
+            fixed(6, heads),
             along(1),
         ],
         out_specs=[
@@ -345,10 +359,10 @@
         ],
         name="states",
     )(
-        values,
+        grouped_value_heads,
         projected_key_query,
         rim,
-        value_kernel_taps.reshape(-1, 2 * lanes),
+        value_kernel_taps,
         key_query_kernel,
         steps,
         facts,
@@ -363,7 +377,7 @@
             by_block(BLOCK, width),
             along(2 * high),
             by_block(BLOCK, BLOCK),
-            fixed(high, 3),
+            fixed(6, heads),
         ],
         out_specs=by_block(BLOCK, 2 * lanes),
         out_shape=jax.ShapeDtypeStruct((positions, 2 * lanes), f32),
@@ -377,8 +391,8 @@
         enter_one,
         enter_two,
         earlier,
-        output_gate_heads.reshape(positions, 2 * lanes),
-        head_norm_gain.reshape(1, 2 * lanes),
+        output_gate_heads,
+        head_norm_gain,
     )
     scratch_shapes = [pltpu.VMEM((sizes[0], lanes), f32), pltpu.VMEM((sizes[1], lanes), f32)]
     if order is None:
@@ -393,8 +407,8 @@
                 per_block(sizes[0], lanes),
                 per_block(sizes[1], lanes),
                 by_block(8, 2 * lanes),
-                by_block(BLOCK, 2 * lanes),
-                fixed(1, 2 * lanes),
+                pl.BlockSpec((BLOCK, 2, lanes), lambda k: (k, 0, 0)),
+                fixed(2, lanes),
             ],
             out_specs=by_block(BLOCK, 2 * lanes),
             out_shape=jax.ShapeDtypeStruct((positions, 2 * lanes), bf16),
@@ -405,36 +419,46 @@
     def whole(*shape):
         return pl.BlockSpec(shape, lambda k, order: (0,) * len(shape))
 
-    def chosen(rows, columns):
-        return pl.BlockSpec((rows, columns), lambda k, order: (order[k], 0))
-
-    def chosen_state(*shape):
-        return pl.BlockSpec((1, *shape), lambda k, order: (order[k],) + (0,) * len(shape))
-
     model_width = output_matrix.shape[2]
-    return pl.pallas_call(
-        functools.partial(projected_kernel, heads, sizes, len(priors), blocks),
-        grid_spec=pltpu.PrefetchScalarGridSpec(
-            num_scalar_prefetch=1,
-            grid=(blocks,),
-            in_specs=[whole(packed_rows, lanes) for _ in priors]
-            + [
-                chosen(BLOCK, 2 * lanes),
-                chosen(BLOCK, width),
-                chosen(BLOCK, BLOCK),
-                chosen_state(sizes[0], lanes),
-                chosen_state(sizes[1], lanes),
-                chosen(8, 2 * lanes),
-                chosen(BLOCK, 2 * lanes),
-                whole(1, 2 * lanes),
-                whole(2 * lanes, model_width),
-            ],
-            out_specs=[whole(BLOCK, model_width)] * blocks,
-            scratch_shapes=scratch_shapes,
-        ),
-        out_shape=[jax.ShapeDtypeStruct((BLOCK, model_width), bf16)] * blocks,
-        name="projected",
-    )(order, *operands, output_matrix.reshape(2 * lanes, model_width))
+    outs = {}
+    for turns in ((3, 2), (1, 0)):
+        count = len(turns)
+
+        def target(k, order, turns=turns):
+            return order[0] ^ jnp.where(k == 0, MASKS[turns[0]], MASKS[turns[1]])
+
+        def chosen(rows, columns, target=target):
+            return pl.BlockSpec((rows, columns), lambda k, order: (target(k, order), 0))
+
+        def chosen_state(*shape, target=target):
+            rest = (0,) * len(shape)
+            return pl.BlockSpec((1, *shape), lambda k, order: (target(k, order), *rest))
+
+        results = pl.pallas_call(
+            functools.partial(projected_kernel, heads, sizes, len(priors), count),
+            grid_spec=pltpu.PrefetchScalarGridSpec(
+                num_scalar_prefetch=1,
+                grid=(count,),
+                in_specs=[whole(packed_rows, lanes) for _ in priors]
+                + [
+                    chosen(BLOCK, 2 * lanes),
+                    chosen(BLOCK, width),
+                    chosen(BLOCK, BLOCK),
+                    chosen_state(sizes[0], lanes),
+                    chosen_state(sizes[1], lanes),
+                    chosen(8, 2 * lanes),
+                    pl.BlockSpec((BLOCK, 2, lanes), lambda k, order, t=target: (t(k, order), 0, 0)),
+                    whole(2, lanes),
+                    whole(2 * lanes, model_width),
+                ],
+                out_specs=[whole(BLOCK, model_width)] * count,
+                scratch_shapes=scratch_shapes,
+            ),
+            out_shape=[jax.ShapeDtypeStruct((BLOCK, model_width), bf16)] * count,
+            name="projected",
+        )(order[None], *operands, output_matrix.reshape(2 * lanes, model_width))
+        outs.update(zip(turns, results))
+    return [outs[turn] for turn in range(blocks)]
 
 
 def routed_experts(
@@ -488,12 +512,13 @@
 
 
 def expert_kernel(region, own_ref, *refs):
-    blocks = refs[:4]
-    keep_ref, send_ref = refs[7:9]
-    gate_ref, up_ref, back_ref, arrived = refs[9:]
+    count = len(refs) - 9
+    blocks = refs[:count]
+    keep_ref, send_ref = refs[count + 3 : count + 5]
+    gate_ref, up_ref, back_ref, arrived = refs[count + 5 :]
     fetches = [
         pltpu.make_async_copy(source, target, arrived.at[i])
-        for i, (source, target) in enumerate(zip(refs[4:7], (gate_ref, up_ref, back_ref)))
+        for i, (source, target) in enumerate(zip(refs[count : count + 3], (gate_ref, up_ref, back_ref)))
     ]
     for fetch in fetches:
         fetch.start()
@@ -513,7 +538,7 @@
         weights.append(
             hits[0:1] * (facts[2:3] + facts[4:5]) + hits[1:2] * (facts[3:4] + facts[5:6])
         )
-    named = jnp.concatenate(named + [jnp.zeros((4, rows), jnp.float32)], axis=0)
+    named = jnp.concatenate(named + named[: max(8 - count, 0)], axis=0)
     inner = jnp.dot(named, before, preferred_element_type=jnp.float32)
     slot = jnp.where(named > 0, inner, -1.0)
     taken = []
@@ -522,7 +547,7 @@
         taken.append(jnp.dot(chosen, block[:, :width], preferred_element_type=jnp.float32))
     taken = jnp.concatenate(taken, axis=0).astype(jnp.bfloat16)
     down = jnp.concatenate(
-        [slot[0:4]] + weights + [jnp.zeros((rows - 8, rows), jnp.float32)], axis=0
+        [slot[0:count]] + weights + [jnp.zeros((rows - 2 * count, rows), jnp.float32)], axis=0
     ).T
     fetches[0].wait()
     gate = jnp.dot(taken, gate_ref[...], preferred_element_type=jnp.float32)
@@ -532,17 +557,18 @@
     fetches[2].wait()
     result = jnp.dot(hidden, back_ref[...], preferred_element_type=jnp.float32)
     place = lax.broadcasted_iota(jnp.int32, (rows, region), 1).astype(jnp.float32)
-    for i in range(4):
+    for i in range(count):
         chosen = (place == down[:, i : i + 1]).astype(jnp.bfloat16)
         spread = jnp.dot(
             chosen,
             result[i * region : (i + 1) * region].astype(jnp.bfloat16),
             preferred_element_type=jnp.float32,
         )
-        out_ref = (keep_ref, send_ref)[i // 2]
-        out_ref[i % 2 * rows : (i % 2 + 1) * rows] = (spread * down[:, 4 + i : 5 + i]).astype(
-            jnp.bfloat16
-        )
+        out_ref = (keep_ref, send_ref)[2 * i // count]
+        first = i % (count // 2) * rows
+        out_ref[first : first + rows] = (
+            spread * down[:, count + i : count + i + 1]
+        ).astype(jnp.bfloat16)
 
 
 def run_expert(blocks, own, gate_weight, up_weight, down_weight, capacity):
@@ -552,9 +578,11 @@
     vmem = pl.BlockSpec(memory_space=pltpu.VMEM)
     return pl.pallas_call(
         functools.partial(expert_kernel, region),
-        in_specs=[pl.BlockSpec(memory_space=pltpu.SMEM)] + [vmem] * 4 + [pl.BlockSpec(memory_space=pl.ANY)] * 3,
+        in_specs=[pl.BlockSpec(memory_space=pltpu.SMEM)]
+        + [vmem] * len(blocks)
+        + [pl.BlockSpec(memory_space=pl.ANY)] * 3,
         out_specs=[vmem] * 2,
-        out_shape=[jax.ShapeDtypeStruct((2 * rows, width), jnp.bfloat16)] * 2,
+        out_shape=[jax.ShapeDtypeStruct((len(blocks) // 2 * rows, width), jnp.bfloat16)] * 2,
         scratch_shapes=[
             pltpu.VMEM((width, hidden), jnp.bfloat16),
             pltpu.VMEM((width, hidden), jnp.bfloat16),
@@ -562,15 +590,17 @@
             pltpu.SemaphoreType.DMA((3,)),
         ],
         cost_estimate=pl.CostEstimate(
-            flops=24 * region * width * hidden,
+            flops=6 * len(blocks) * region * width * hidden,
             bytes_accessed=6 * width * hidden,
-            transcendentals=4 * region * hidden,
+            transcendentals=len(blocks) * region * hidden,
         ),
         name="expert",
     )(own[None], *blocks, gate_weight, up_weight, down_weight)
 
 
 def added(block, *received):
+    if len(received) == 1:
+        return block + received[0]
     total = block.astype(jnp.float32)
     for other in received:
         if other is not None:
@@ -614,7 +644,7 @@
 ENDS = [(0, 3), (3, 0)]
 OUTWARD = [(1, 0), (2, 3)]
 INWARD = [(0, 1), (3, 2)]
-ARRIVALS = [[0, 1, 3, 2], [1, 0, 2, 3], [2, 3, 1, 0], [3, 2, 0, 1]]
+MASKS = (0, 1, 3, 2)
 
 
 def line_sum(parts):
@@ -673,31 +703,31 @@
             far.append(swapped(blocks[turn], 2))
         near_other.append(swapped(blocks[turn], 1))
         far_other.append(swapped(far[turn], 1))
-    near_sums, far_sums = [], []
-    for turn in range(4):
-        keep, send = run_expert(
-            [blocks[turn], far[turn], near_other[turn], far_other[turn]],
-            mine,
-            gate_weight,
-            up_weight,
-            down_weight,
-            capacity,
-        )
+    experts = (mine, gate_weight, up_weight, down_weight, capacity)
+    near, crossed = [], []
+    for turns in ((0, 1), (2,), (3,)):
+        kept = [b for turn in turns for b in (blocks[turn], far[turn])]
+        sent = [b for turn in turns for b in (near_other[turn], far_other[turn])]
+        keep, send = run_expert(kept + sent, *experts)
         back = swapped(send, 1)
-        near_sums.append((keep[:rows], back[:rows]))
-        if turn == 3:
-            near_last = near_added(keep, back)
-        far_sums.append(added(keep[rows:], back[rows:]))
-    crossed = [swapped(far_sums[turn], 2) for turn in range(4)]
-    parts = [None, added(*near_sums[1], crossed[1])]
-    parts.append(lax.optimization_barrier(added(*near_sums[2], crossed[2])))
+        fenced = lax.optimization_barrier((keep, back))
+        for i, turn in enumerate(turns):
+            here = slice(2 * i * rows, (2 * i + 1) * rows)
+            beyond = slice((2 * i + 1) * rows, 2 * (i + 1) * rows)
+            near.append((fenced[0][here], fenced[1][here]))
+            crossed.append(swapped(added(keep[beyond], back[beyond]), 2))
+    near_last = near_added(keep, back)
+    parts = [None]
+    for turn in (1, 2):
+        parts.append(added(*near[turn], crossed[turn]))
+    parts[2] = lax.optimization_barrier(parts[2])
     parts.append(lax.optimization_barrier(added(near_last, crossed[3])))
     sums = line_sum(parts)[1:]
     return pl.pallas_call(
         final_kernel,
         out_shape=jax.ShapeDtypeStruct(stream.shape, jnp.bfloat16),
         name="final",
-    )(stream, *near_sums[0], crossed[0], *sums)
+    )(stream, *near[0], crossed[0], *sums)
 
 
 def local(
@@ -723,7 +753,7 @@
 ):
     lane_width = grouped_value_heads.shape[2]
     dense = lax.axis_size("sp") == 4 and lax.axis_size("tp") == 4
-    order = jnp.asarray(ARRIVALS, jnp.int32)[lax.axis_index("tp")] if dense else None
+    order = lax.axis_index("tp").astype(jnp.int32) if dense else None
     mixed_heads = mixed_rows(
         grouped_value_heads,
         output_gate_heads,

time: 285 us -> 252 us (0.88)
  waiting for transfers between devices: 129 us -> 75.3 us
  starting transfers between devices: 52.6 us -> 88.5 us
  local copies, waits for them, and re-layouts: 19 us -> 7.01 us
    ppermute x20 -> x19, waiting for transfers between devices: 63.3 us -> 34.6 us  [swapped(): lax.ppermute(array, 'sp', [(i, i ^ bit) for i in range(lax.axis_size('sp'...]
    ppermute x20 -> x19, starting transfers between devices: 7.27 us -> 25.8 us  [swapped(): lax.ppermute(array, 'sp', [(i, i ^ bit) for i in range(lax.axis_size('sp'...]
    ppermute x2, starting transfers between devices: 11.4 us -> 26.4 us  [line_sum(): pair = lax.ppermute(added(parts[1], middle), 'tp', SWAPS)]
    convert_element_type x10 -> x1, other arithmetic: 13 us -> 1.28 us  [added(): return total.astype(jnp.bfloat16)]
    add x0 -> x8, other arithmetic: none -> 9.47 us  [added(): return block + received[0]]
    ppermute x2, waiting for transfers between devices: 7.49 us -> 0.7 us  [line_sum(): inward = lax.ppermute(parts[3], 'tp', INWARD)]
    ppermute x1, waiting for transfers between devices: 12.5 us -> 6.71 us  [dense_experts(): outer_two = lax.ppermute(second, 'tp', OUTWARD)]
    ppermute x2, waiting for transfers between devices: 5.31 us -> 0.01 us  [line_sum(): ends = lax.ppermute(parts[2], 'tp', ENDS)]
  transfers between devices with their start and end apart: 38 -> 37, of which waited for: 13 -> 11; matrix products, arithmetic and copies ran while one was open for 10% -> 5% of each run, Pallas kernels for 16% -> 19%
where the time goes in v1:
time: 252 us; the launch traced here: 251 us
  starting transfers between devices  88.5 us (35%)
  waiting for transfers between devices  75.3 us (30%)
  Pallas kernels  67.7 us (27%)
  other arithmetic  12.1 us (5%)
  local copies, waits for them, and re-layouts  7.01 us (3%)
    ppermute x19, waiting for transfers between devices, swapped(): lax.ppermute(array, 'sp', [(i, i ^ bit) for i in range(lax.axis_size('sp'...  34.6 us
    pallas_call x3, Pallas kernels, run_expert(): pl.pallas_call(functools.partial(expert_kernel, region), in_specs=[pl.Blo...  34.4 us
    ppermute x2, starting transfers between devices, line_sum(): pair = lax.ppermute(added(parts[1], middle), 'tp', SWAPS)  26.4 us
    ppermute x19, starting transfers between devices, swapped(): lax.ppermute(array, 'sp', [(i, i ^ bit) for i in range(lax.axis_size('sp'...  25.8 us
    ppermute x2, waiting for transfers between devices, line_sum(): pair = lax.ppermute(added(parts[1], middle), 'tp', SWAPS)  15.2 us
    pallas_call x2, Pallas kernels, mixed_rows(): pl.pallas_call(functools.partial(projected_kernel, heads, sizes, len(prio...  13.2 us
    ppermute x4, starting transfers between devices, passed_along(): return lax.ppermute(shard, axis, pairs)  11.8 us
    ppermute x1, waiting for transfers between devices, dense_experts(): second = lax.ppermute(normed, 'tp', MIDDLE + ENDS)  11.6 us
  transfers between devices with their start and end apart: 37, of which 11 were waited for; matrix products, arithmetic and copies ran while one was open for 5% of the time, Pallas kernels for 19%

profile of v1, /device:TPU:0, one launch (start us, length us, event | category | flops | bytes accessed | tf_op | source)
XLA Modules:
  0.0 251.1 jit_solution(10406540318258817342)
XLA Ops:
  5.7 7.0 %states.1 = (bf16[512,512]{1,0:T(8,128)(2,1)}, bf16[512,384]{1,0:T(8,128)(2,1)}, f32[16,512]{1,0:T(8,128)}, f32[512,128]{1,0:T(8,128)}, f32[4,64,256]{2,1,0:T(8,...) custom-call(bf16[512,2,256]{2,1,0:T(2,128)(2,1)} %values_ref.1, ...), custom_call_target="tpu_custom_call" | custom-call | tf_op jit(solution)/shard_map/states/pallas_call | solution.py:321
  12.8 4.5 %collective-permute-start.1 = (bf16[208,256]{1,0:T(8,128)(2,1)}, bf16[208,256]{1,0:T(8,128)(2,1)S(1)}, u32[]{:S(2)}, u32[]{:S(2)}) collective-permute-start(bf16[208,256]{1,0:T(8,128)(2,1)} %get-tuple-element.29), channel_id=1, source_target_pairs={{0,4},{4,8},{8,12},{1,5},{5,9},{9,13},{2,6},{6,10},{10,14},{3,7},{... | collective-permute-start | bytes 319496 | tf_op jit(solution)/shard_map/ppermute | solution.py:23
  22.2 4.7 %near.1.refs_3_ = f32[512,512]{1,0:T(8,128)} custom-call(bf16[512,512]{1,0:T(8,128)(2,1)} %get-tuple-element.30.x_ref, bf16[512,384]{1,0:T(8,128)(2,1)} %get-tuple-element.31.rows_ref.refs_4_, f32[16,512]{1,0:T(8,128)} %get-tuple-element.32.across_ref, f32[512,128]{1,0:T(8,128)} %get-tuple-element.33.down_ref.refs_5_, f32[6,4]{1,0:T(8,128)} %pad_maximum_fusion.1.facts_ref), custom_call_target="tpu_custom_call" | custom-call | tf_op jit(solution)/shard_map/near/pallas_call | solution.py:372
  27.7 6.6 %projected.3 = (bf16[128,2048]{1,0:T(8,128)(2,1)}, bf16[128,2048]{1,0:T(8,128)(2,1)}) custom-call(s32[1]{0:T(128)} %bitcast.order_ref, bf16[208,256]{1,0:T(8,128)(2,1)} %copy-done.19, bf16[208,256]{1,0:T(8,128)(2,1)} %copy-done.20, bf16[208,256]{1,0:T(8,128)(2,1)} %copy-done.21, f32[512,512]{1,0:T(8,128)} %near.1.refs_3_, ...), custom_call_target="tpu_custom_call" | custom-call | tf_op jit(solution)/shard_map/projected/pallas_call | solution.py:437
  38.5 4.5 %collective-permute-start.4 = (bf16[128,2048]{1,0:T(8,128)(2,1)}, bf16[128,2048]{1,0:T(8,128)(2,1)S(1)}, u32[]{:S(2)}, u32[]{:S(2)}) collective-permute-start(bf16[128,2048]{1,0:T(8,128)(2,1)} %get-tuple-element.38), channel_id=1, source_target_pairs={{0,3},{3,0},{4,7},{7,4},{8,11},{11,8},{12,15},{15,12},{16,19},{19,... | collective-permute-start | bytes 1572872 | tf_op jit(solution)/shard_map/ppermute | solution.py:651
  43.0 6.6 %projected.2 = (bf16[128,2048]{1,0:T(8,128)(2,1)}, bf16[128,2048]{1,0:T(8,128)(2,1)}) custom-call(s32[1]{0:T(128)} %bitcast.order_ref, bf16[208,256]{1,0:T(8,128)(2,1)} %copy-done.19, bf16[208,256]{1,0:T(8,128)(2,1)} %copy-done.20, bf16[208,256]{1,0:T(8,128)(2,1)} %copy-done.21, f32[512,512]{1,0:T(8,128)} %near.1.refs_3_, ...), custom_call_target="tpu_custom_call" | custom-call | tf_op jit(solution)/shard_map/projected/pallas_call | solution.py:437
  52.4 12.4 %collective-permute-start.6 = (bf16[128,2048]{1,0:T(8,128)(2,1)S(1)}, bf16[128,2048]{1,0:T(8,128)(2,1)S(1)}, u32[]{:S(2)}, u32[]{:S(2)}) collective-permute-start(bf16[128,2048]{1,0:T(8,128)(2,1)S(1)} %add.41), channel_id=1, source_target_pairs={{0,1},{1,0},{2,3},{3,2},{4,5},{5,4},{6,7},{7,6},{8,9},{9,8},{10,11... | collective-permute-start | bytes 1572872 | tf_op jit(solution)/shard_map/ppermute | solution.py:654
  65.6 8.1 %collective-permute-done.6.two_ref = bf16[128,2048]{1,0:T(8,128)(2,1)S(1)} collective-permute-done((bf16[128,2048]{1,0:T(8,128)(2,1)S(1)}, bf16[128,2048]{1,0:T(8,128)(2,1)S(1)}, u32[]{:S(2)}, u32[]{:S(2)}) %collective-permute-start.6) | collective-permute-done | bytes 524320 | tf_op jit(solution)/shard_map/ppermute | solution.py:654
  81.2 4.5 %collective-permute-start.9 = (bf16[128,2176]{1,0:T(8,128)(2,1)}, bf16[128,2176]{1,0:T(8,128)(2,1)}, u32[]{:S(2)}, u32[]{:S(2)}) collective-permute-start(bf16[128,2176]{1,0:T(8,128)(2,1)} %get-tuple-element.42.refs_0_), channel_id=1, source_target_pairs={{0,8},{4,12},{8,0},{12,4},{1,9},{5,13},{9,1},{13,5},{2,10},{6,14},... | collective-permute-start | bytes 1671176 | tf_op jit(solution)/shard_map/ppermute | solution.py:511
  85.8 6.4 %collective-permute-done.10.refs_2_ = bf16[128,2176]{1,0:T(8,128)(2,1)} collective-permute-done((bf16[128,2176]{1,0:T(8,128)(2,1)}, bf16[128,2176]{1,0:T(8,128)(2,1)}, u32[]{:S(2)}, u32[]{:S(2)}) %collective-permute-start.10) | collective-permute-done | bytes 557088 | tf_op jit(solution)/shard_map/ppermute | solution.py:693
  92.9 11.6 %collective-permute-done.18.refs_0_ = bf16[128,2176]{1,0:T(8,128)(2,1)S(1)} collective-permute-done((bf16[128,2176]{1,0:T(8,128)(2,1)}, bf16[128,2176]{1,0:T(8,128)(2,1)S(1)}, u32[]{:S(2)}, u32[]{:S(2)}) %collective-permute-start.18) | collective-permute-done | bytes 557088 | tf_op jit(solution)/shard_map/ppermute | solution.py:694
  106.1 5.5 %collective-permute-start.19 = (bf16[128,2176]{1,0:T(8,128)(2,1)S(1)}, bf16[128,2176]{1,0:T(8,128)(2,1)S(1)}, u32[]{:S(2)}, u32[]{:S(2)}) collective-permute-start(bf16[128,2176]{1,0:T(8,128)(2,1)S(1)} %collective-permute-done.18.refs_0_), channel_id=1, source_target_pairs={{0,8},{4,12},{8,0},{12,4},{1,9},{5,13},{9,1},{13,5},{2,10},{6,14},... | collective-permute-start | bytes 1671176 | tf_op jit(solution)/shard_map/ppermute | solution.py:511
  111.8 6.7 %collective-permute-done.27 = bf16[128,2176]{1,0:T(8,128)(2,1)S(1)} collective-permute-done((bf16[128,2176]{1,0:T(8,128)(2,1)S(1)}, bf16[128,2176]{1,0:T(8,128)(2,1)S(1)}, u32[]{:S(2)}, u32[]{:S(2)}) %collective-permute-start.27) | collective-permute-done | bytes 557088 | tf_op jit(solution)/shard_map/ppermute | solution.py:696
  118.6 6.5 %collective-permute-start.28 = (bf16[128,2176]{1,0:T(8,128)(2,1)S(1)}, bf16[128,2176]{1,0:T(8,128)(2,1)S(1)}, u32[]{:S(2)}, u32[]{:S(2)}) collective-permute-start(bf16[128,2176]{1,0:T(8,128)(2,1)S(1)} %broadcast_select_fusion.refs_0_), channel_id=1, source_target_pairs={{0,8},{4,12},{8,0},{12,4},{1,9},{5,13},{9,1},{13,5},{2,10},{6,14},... | collective-permute-start | bytes 1671176 | tf_op jit(solution)/shard_map/ppermute | solution.py:511
  125.1 12.0 %collective-permute-done.11.refs_3_ = bf16[128,2176]{1,0:T(8,128)(2,1)} collective-permute-done((bf16[128,2176]{1,0:T(8,128)(2,1)}, bf16[128,2176]{1,0:T(8,128)(2,1)}, u32[]{:S(2)}, u32[]{:S(2)}) %collective-permute-start.11) | collective-permute-done | bytes 557088 | tf_op jit(solution)/shard_map/ppermute | solution.py:511
  138.1 10.5 %collective-permute-done.28.refs_1_ = bf16[128,2176]{1,0:T(8,128)(2,1)S(1)} collective-permute-done((bf16[128,2176]{1,0:T(8,128)(2,1)S(1)}, bf16[128,2176]{1,0:T(8,128)(2,1)S(1)}, u32[]{:S(2)}, u32[]{:S(2)}) %collective-permute-start.28) | collective-permute-done | bytes 557088 | tf_op jit(solution)/shard_map/ppermute | solution.py:511
  148.7 15.0 %expert.3 = (bf16[512,2048]{1,0:T(8,128)(2,1)}, bf16[512,2048]{1,0:T(8,128)(2,1)}) custom-call(s32[1]{0:T(128)} %bitcast.5.own_ref, bf16[128,2176]{1,0:T(8,128)(2,1)} %get-tuple-element.42.refs_0_, bf16[128,2176]{1,0:T(8,128)(2,1)} %collective-permute-done.9.refs_1_, bf16[128,2176]{1,0:T(8,128)(2,1)} %collective-permute-done.10.refs_2_, ...), custom_call_target="tpu_custom_call" | custom-call | flops 7247757312 | bytes 12582912 | tf_op jit(solution)/shard_map/expert/pallas_call | solution.py:579
  165.0 9.7 %expert.5 = (bf16[256,2048]{1,0:T(8,128)(2,1)}, bf16[256,2048]{1,0:T(8,128)(2,1)}) custom-call(s32[1]{0:T(128)} %bitcast.5.own_ref, bf16[128,2176]{1,0:T(8,128)(2,1)} %copy-done.2, bf16[128,2176]{1,0:T(8,128)(2,1)} %copy-done.9, bf16[128,2176]{1,0:T(8,128)(2,1)} %copy-done.10, bf16[128,2176]{1,0:T(8,128)(2,1)} %collective-permute-done.30.refs_3_, ...), custom_call_target="tpu_custom_call" | custom-call | flops 3623878656 | bytes 12582912 | tf_op jit(solution)/shard_map/expert/pallas_call | solution.py:579
  175.0 9.6 %expert.4 = (bf16[256,2048]{1,0:T(8,128)(2,1)}, bf16[256,2048]{1,0:T(8,128)(2,1)}) custom-call(s32[1]{0:T(128)} %bitcast.5.own_ref, bf16[128,2176]{1,0:T(8,128)(2,1)} %copy-done.7, bf16[128,2176]{1,0:T(8,128)(2,1)} %copy-done.8, bf16[128,2176]{1,0:T(8,128)(2,1)} %collective-permute-done.20.refs_2_, bf16[128,2176]{1,0:T(8,128)(2,1)} %collective-permute-done.21.refs_3_, ...), custom_call_target="tpu_custom_call" | custom-call | flops 3623878656 | bytes 12582912 | tf_op jit(solution)/shard_map/expert/pallas_call | solution.py:579
  194.4 6.6 %collective-permute-done.32 = bf16[128,2048]{1,0:T(8,128)(2,1)} collective-permute-done((bf16[128,2048]{1,0:T(8,128)(2,1)}, bf16[128,2048]{1,0:T(8,128)(2,1)}, u32[]{:S(2)}, u32[]{:S(2)}) %collective-permute-start.32) | collective-permute-done | bytes 524320 | tf_op jit(solution)/shard_map/ppermute | solution.py:511
  202.3 4.6 %collective-permute-start.35 = (bf16[128,2048]{1,0:T(8,128)(2,1)S(1)}, bf16[128,2048]{1,0:T(8,128)(2,1)S(1)}, u32[]{:S(2)}, u32[]{:S(2)}) collective-permute-start(bf16[128,2048]{1,0:T(8,128)(2,1)S(1)} %add.51), channel_id=1, source_target_pairs={{0,1},{3,2},{4,5},{7,6},{8,9},{11,10},{12,13},{15,14},{16,17},{19,... | collective-permute-start | bytes 1572872 | tf_op jit(solution)/shard_map/ppermute | solution.py:653
  219.4 3.9 %collective-permute-done.25 = bf16[128,2048]{1,0:T(8,128)(2,1)S(1)} collective-permute-done((bf16[128,2048]{1,0:T(8,128)(2,1)S(1)}, bf16[128,2048]{1,0:T(8,128)(2,1)S(1)}, u32[]{:S(2)}, u32[]{:S(2)}) %collective-permute-start.25) | collective-permute-done | bytes 524320 | tf_op jit(solution)/shard_map/ppermute | solution.py:511
  226.0 14.0 %collective-permute-start.34 = (bf16[128,2048]{1,0:T(8,128)(2,1)S(1)}, bf16[128,2048]{1,0:T(8,128)(2,1)S(1)}, u32[]{:S(2)}, u32[]{:S(2)}) collective-permute-start(bf16[128,2048]{1,0:T(8,128)(2,1)S(1)} %get-tuple-element.57), channel_id=1, source_target_pairs={{0,1},{1,0},{2,3},{3,2},{4,5},{5,4},{6,7},{7,6},{8,9},{9,8},{10,11... | collective-permute-start | bytes 1572872 | tf_op jit(solution)/shard_map/ppermute | solution.py:654
  240.0 7.1 %collective-permute-done.34.refs_4_ = bf16[128,2048]{1,0:T(8,128)(2,1)S(1)} collective-permute-done((bf16[128,2048]{1,0:T(8,128)(2,1)S(1)}, bf16[128,2048]{1,0:T(8,128)(2,1)S(1)}, u32[]{:S(2)}, u32[]{:S(2)}) %collective-permute-start.34) | collective-permute-done | bytes 524320 | tf_op jit(solution)/shard_map/ppermute | solution.py:654
  (130 shorter events, 61.7 us)
Async XLA Ops:
  34.3 16.1 %collective-permute-start.7 = (bf16[128,2048]{1,0:T(8,128)(2,1)}, bf16[128,2048]{1,0:T(8,128)(2,1)S(1)}, u32[]{:S(2)}, u32[]{:S(2)}) collective-permute-start(bf16[128,2048]{1,0:T(8,128)(2,1)} %get-tuple-element.40), channel_id=1, source_target_pairs={{0,1},{3,2},{4,5},{7,6},{8,9},{11,10},{12,13},{15,14},{16,17},{19,... | collective-permute-start | bytes 1572872 | tf_op jit(solution)/shard_map/ppermute | solution.py:653
  38.5 27.1 %collective-permute-start.4 = (bf16[128,2048]{1,0:T(8,128)(2,1)}, bf16[128,2048]{1,0:T(8,128)(2,1)S(1)}, u32[]{:S(2)}, u32[]{:S(2)}) collective-permute-start(bf16[128,2048]{1,0:T(8,128)(2,1)} %get-tuple-element.38), channel_id=1, source_target_pairs={{0,3},{3,0},{4,7},{7,4},{8,11},{11,8},{12,15},{15,12},{16,19},{19,... | collective-permute-start | bytes 1572872 | tf_op jit(solution)/shard_map/ppermute | solution.py:651
  52.4 21.3 %collective-permute-start.6 = (bf16[128,2048]{1,0:T(8,128)(2,1)S(1)}, bf16[128,2048]{1,0:T(8,128)(2,1)S(1)}, u32[]{:S(2)}, u32[]{:S(2)}) collective-permute-start(bf16[128,2048]{1,0:T(8,128)(2,1)S(1)} %add.41), channel_id=1, source_target_pairs={{0,1},{1,0},{2,3},{3,2},{4,5},{5,4},{6,7},{7,6},{8,9},{9,8},{10,11... | collective-permute-start | bytes 1572872 | tf_op jit(solution)/shard_map/ppermute | solution.py:654
  78.5 26.0 %collective-permute-start.18 = (bf16[128,2176]{1,0:T(8,128)(2,1)}, bf16[128,2176]{1,0:T(8,128)(2,1)S(1)}, u32[]{:S(2)}, u32[]{:S(2)}) collective-permute-start(bf16[128,2176]{1,0:T(8,128)(2,1)} %get-tuple-element.42.refs_0_), channel_id=1, source_target_pairs={{1,2},{2,1},{0,3},{3,0},{5,6},{6,5},{4,7},{7,4},{9,10},{10,9},{8,1... | collective-permute-start | bytes 1671176 | tf_op jit(solution)/shard_map/ppermute | solution.py:694
  81.2 30.4 %collective-permute-start.9 = (bf16[128,2176]{1,0:T(8,128)(2,1)}, bf16[128,2176]{1,0:T(8,128)(2,1)}, u32[]{:S(2)}, u32[]{:S(2)}) collective-permute-start(bf16[128,2176]{1,0:T(8,128)(2,1)} %get-tuple-element.42.refs_0_), channel_id=1, source_target_pairs={{0,8},{4,12},{8,0},{12,4},{1,9},{5,13},{9,1},{13,5},{2,10},{6,14},... | collective-permute-start | bytes 1671176 | tf_op jit(solution)/shard_map/ppermute | solution.py:511
  92.2 19.5 %collective-permute-start.26 = (bf16[128,2176]{1,0:T(8,128)(2,1)}, bf16[128,2176]{1,0:T(8,128)(2,1)S(1)}, u32[]{:S(2)}, u32[]{:S(2)}) collective-permute-start(bf16[128,2176]{1,0:T(8,128)(2,1)} %collective-permute-done.10.refs_2_), channel_id=1, source_target_pairs={{1,2},{2,1},{5,6},{6,5},{9,10},{10,9},{13,14},{14,13},{17,18},{18,... | collective-permute-start | bytes 1671176 | tf_op jit(solution)/shard_map/ppermute | solution.py:695
  106.1 31.0 %collective-permute-start.19 = (bf16[128,2176]{1,0:T(8,128)(2,1)S(1)}, bf16[128,2176]{1,0:T(8,128)(2,1)S(1)}, u32[]{:S(2)}, u32[]{:S(2)}) collective-permute-start(bf16[128,2176]{1,0:T(8,128)(2,1)S(1)} %collective-permute-done.18.refs_0_), channel_id=1, source_target_pairs={{0,8},{4,12},{8,0},{12,4},{1,9},{5,13},{9,1},{13,5},{2,10},{6,14},... | collective-permute-start | bytes 1671176 | tf_op jit(solution)/shard_map/ppermute | solution.py:511
  111.6 25.5 %collective-permute-start.11 = (bf16[128,2176]{1,0:T(8,128)(2,1)}, bf16[128,2176]{1,0:T(8,128)(2,1)}, u32[]{:S(2)}, u32[]{:S(2)}) collective-permute-start(bf16[128,2176]{1,0:T(8,128)(2,1)} %collective-permute-done.10.refs_2_), channel_id=1, source_target_pairs={{0,8},{4,12},{8,0},{12,4},{1,9},{5,13},{9,1},{13,5},{2,10},{6,14},... | collective-permute-start | bytes 1671176 | tf_op jit(solution)/shard_map/ppermute | solution.py:511
  111.7 26.0 %collective-permute-start.14 = (bf16[128,2176]{1,0:T(8,128)(2,1)}, bf16[128,2176]{1,0:T(8,128)(2,1)}, u32[]{:S(2)}, u32[]{:S(2)}) collective-permute-start(bf16[128,2176]{1,0:T(8,128)(2,1)} %collective-permute-done.10.refs_2_), channel_id=1, source_target_pairs={{0,4},{4,0},{8,12},{12,8},{1,5},{5,1},{9,13},{13,9},{2,6},{6,2},{1... | collective-permute-start | bytes 1671176 | tf_op jit(solution)/shard_map/ppermute | solution.py:511
  118.5 19.1 %collective-permute-start.13 = (bf16[128,2176]{1,0:T(8,128)(2,1)}, bf16[128,2176]{1,0:T(8,128)(2,1)}, u32[]{:S(2)}, u32[]{:S(2)}) collective-permute-start(bf16[128,2176]{1,0:T(8,128)(2,1)} %collective-permute-done.9.refs_1_), channel_id=1, source_target_pairs={{0,4},{4,0},{8,12},{12,8},{1,5},{5,1},{9,13},{13,9},{2,6},{6,2},{1... | collective-permute-start | bytes 1671176 | tf_op jit(solution)/shard_map/ppermute | solution.py:511
  118.6 30.1 %collective-permute-start.28 = (bf16[128,2176]{1,0:T(8,128)(2,1)S(1)}, bf16[128,2176]{1,0:T(8,128)(2,1)S(1)}, u32[]{:S(2)}, u32[]{:S(2)}) collective-permute-start(bf16[128,2176]{1,0:T(8,128)(2,1)S(1)} %broadcast_select_fusion.refs_0_), channel_id=1, source_target_pairs={{0,8},{4,12},{8,0},{12,4},{1,9},{5,13},{9,1},{13,5},{2,10},{6,14},... | collective-permute-start | bytes 1671176 | tf_op jit(solution)/shard_map/ppermute | solution.py:511
  137.1 37.9 %collective-permute-start.20 = (bf16[128,2176]{1,0:T(8,128)(2,1)S(1)}, bf16[128,2176]{1,0:T(8,128)(2,1)}, u32[]{:S(2)}, u32[]{:S(2)}) collective-permute-start(bf16[128,2176]{1,0:T(8,128)(2,1)S(1)} %collective-permute-done.18.refs_0_), channel_id=1, source_target_pairs={{0,4},{4,0},{8,12},{12,8},{1,5},{5,1},{9,13},{13,9},{2,6},{6,2},{1... | collective-permute-start | bytes 1671176 | tf_op jit(solution)/shard_map/ppermute | solution.py:511
  137.6 26.5 %collective-permute-start.29 = (bf16[128,2176]{1,0:T(8,128)(2,1)S(1)}, bf16[128,2176]{1,0:T(8,128)(2,1)S(1)}, u32[]{:S(2)}, u32[]{:S(2)}) collective-permute-start(bf16[128,2176]{1,0:T(8,128)(2,1)S(1)} %broadcast_select_fusion.refs_0_), channel_id=1, source_target_pairs={{0,4},{4,0},{8,12},{12,8},{1,5},{5,1},{9,13},{13,9},{2,6},{6,2},{1... | collective-permute-start | bytes 1671176 | tf_op jit(solution)/shard_map/ppermute | solution.py:511
  137.7 37.3 %collective-permute-start.21 = (bf16[128,2176]{1,0:T(8,128)(2,1)S(1)}, bf16[128,2176]{1,0:T(8,128)(2,1)}, u32[]{:S(2)}, u32[]{:S(2)}) collective-permute-start(bf16[128,2176]{1,0:T(8,128)(2,1)S(1)} %collective-permute-done.19.refs_1_), channel_id=1, source_target_pairs={{0,4},{4,0},{8,12},{12,8},{1,5},{5,1},{9,13},{13,9},{2,6},{6,2},{1... | collective-permute-start | bytes 1671176 | tf_op jit(solution)/shard_map/ppermute | solution.py:511
  148.7 15.5 %collective-permute-start.30 = (bf16[128,2176]{1,0:T(8,128)(2,1)S(1)}, bf16[128,2176]{1,0:T(8,128)(2,1)}, u32[]{:S(2)}, u32[]{:S(2)}) collective-permute-start(bf16[128,2176]{1,0:T(8,128)(2,1)S(1)} %collective-permute-done.28.refs_1_), channel_id=1, source_target_pairs={{0,4},{4,0},{8,12},{12,8},{1,5},{5,1},{9,13},{13,9},{2,6},{6,2},{1... | collective-permute-start | bytes 1671176 | tf_op jit(solution)/shard_map/ppermute | solution.py:511
  163.8 43.2 %collective-permute-start.16 = (bf16[512,2048]{1,0:T(8,128)(2,1)}, bf16[512,2048]{1,0:T(8,128)(2,1)}, u32[]{:S(2)}, u32[]{:S(2)}) collective-permute-start(bf16[512,2048]{1,0:T(8,128)(2,1)} %get-tuple-element.44), channel_id=1, source_target_pairs={{0,4},{4,0},{8,12},{12,8},{1,5},{5,1},{9,13},{13,9},{2,6},{6,2},{1... | collective-permute-start | bytes 6291464 | tf_op jit(solution)/shard_map/ppermute | solution.py:511
  185.9 15.1 %collective-permute-start.32 = (bf16[128,2048]{1,0:T(8,128)(2,1)}, bf16[128,2048]{1,0:T(8,128)(2,1)}, u32[]{:S(2)}, u32[]{:S(2)}) collective-permute-start(bf16[128,2048]{1,0:T(8,128)(2,1)} %slice_add_fusion), channel_id=1, source_target_pairs={{0,8},{4,12},{8,0},{12,4},{1,9},{5,13},{9,1},{13,5},{2,10},{6,14},... | collective-permute-start | bytes 1572872 | tf_op jit(solution)/shard_map/ppermute | solution.py:511
  190.6 21.6 %collective-permute-start.23 = (bf16[128,2048]{1,0:T(8,128)(2,1)}, bf16[128,2048]{1,0:T(8,128)(2,1)}, u32[]{:S(2)}, u32[]{:S(2)}) collective-permute-start(bf16[128,2048]{1,0:T(8,128)(2,1)} %slice_add_fusion.2), channel_id=1, source_target_pairs={{0,8},{4,12},{8,0},{12,4},{1,9},{5,13},{9,1},{13,5},{2,10},{6,14},... | collective-permute-start | bytes 1572872 | tf_op jit(solution)/shard_map/ppermute | solution.py:511
  202.3 16.3 %collective-permute-start.35 = (bf16[128,2048]{1,0:T(8,128)(2,1)S(1)}, bf16[128,2048]{1,0:T(8,128)(2,1)S(1)}, u32[]{:S(2)}, u32[]{:S(2)}) collective-permute-start(bf16[128,2048]{1,0:T(8,128)(2,1)S(1)} %add.51), channel_id=1, source_target_pairs={{0,1},{3,2},{4,5},{7,6},{8,9},{11,10},{12,13},{15,14},{16,17},{19,... | collective-permute-start | bytes 1572872 | tf_op jit(solution)/shard_map/ppermute | solution.py:653
  208.3 15.1 %collective-permute-start.25 = (bf16[128,2048]{1,0:T(8,128)(2,1)S(1)}, bf16[128,2048]{1,0:T(8,128)(2,1)S(1)}, u32[]{:S(2)}, u32[]{:S(2)}) collective-permute-start(bf16[128,2048]{1,0:T(8,128)(2,1)S(1)} %get-tuple-element.55), channel_id=1, source_target_pairs={{0,8},{4,12},{8,0},{12,4},{1,9},{5,13},{9,1},{13,5},{2,10},{6,14},... | collective-permute-start | bytes 1572872 | tf_op jit(solution)/shard_map/ppermute | solution.py:511
  213.5 26.4 %collective-permute-start.24 = (bf16[128,2048]{1,0:T(8,128)(2,1)S(1)}, bf16[128,2048]{1,0:T(8,128)(2,1)S(1)}, u32[]{:S(2)}, u32[]{:S(2)}) collective-permute-start(bf16[128,2048]{1,0:T(8,128)(2,1)S(1)} %add_convert_fusion.1), channel_id=1, source_target_pairs={{0,3},{3,0},{4,7},{7,4},{8,11},{11,8},{12,15},{15,12},{16,19},{19,... | collective-permute-start | bytes 1572872 | tf_op jit(solution)/shard_map/ppermute | solution.py:651
  216.8 23.2 %collective-permute-start.17 = (bf16[128,2048]{1,0:T(8,128)(2,1)S(1)}, bf16[128,2048]{1,0:T(8,128)(2,1)S(1)}, u32[]{:S(2)}, u32[]{:S(2)}) collective-permute-start(bf16[128,2048]{1,0:T(8,128)(2,1)S(1)} %get-tuple-element.56), channel_id=1, source_target_pairs={{0,8},{4,12},{8,0},{12,4},{1,9},{5,13},{9,1},{13,5},{2,10},{6,14},... | collective-permute-start | bytes 1572872 | tf_op jit(solution)/shard_map/ppermute | solution.py:511
  218.7 21.2 %collective-permute-start.36 = (bf16[128,2048]{1,0:T(8,128)(2,1)S(1)}, bf16[128,2048]{1,0:T(8,128)(2,1)S(1)}, u32[]{:S(2)}, u32[]{:S(2)}) collective-permute-start(bf16[128,2048]{1,0:T(8,128)(2,1)S(1)} %add.53), channel_id=1, source_target_pairs={{1,2},{2,1},{5,6},{6,5},{9,10},{10,9},{13,14},{14,13},{17,18},{18,... | collective-permute-start | bytes 1572872 | tf_op jit(solution)/shard_map/ppermute | solution.py:655
  226.0 21.1 %collective-permute-start.34 = (bf16[128,2048]{1,0:T(8,128)(2,1)S(1)}, bf16[128,2048]{1,0:T(8,128)(2,1)S(1)}, u32[]{:S(2)}, u32[]{:S(2)}) collective-permute-start(bf16[128,2048]{1,0:T(8,128)(2,1)S(1)} %get-tuple-element.57), channel_id=1, source_target_pairs={{0,1},{1,0},{2,3},{3,2},{4,5},{5,4},{6,7},{7,6},{8,9},{9,8},{10,11... | collective-permute-start | bytes 1572872 | tf_op jit(solution)/shard_map/ppermute | solution.py:654
  (38 other events, 443.0 us)

commit v2 on v1

--- a/solution.py
+++ b/solution.py
@@ -369,23 +369,9 @@
         position_extra_decay[None],
     )
     priors = [passed_along(packed, "sp", by) for by in range(1, lax.axis_size("sp"))]
-    near = pl.pallas_call(
-        functools.partial(near_kernel, heads, sizes),
-        grid=(blocks,),
-        in_specs=[
-            by_block(BLOCK, 2 * lanes),
-            by_block(BLOCK, width),
-            along(2 * high),
-            by_block(BLOCK, BLOCK),
-            fixed(6, heads),
-        ],
-        out_specs=by_block(BLOCK, 2 * lanes),
-        out_shape=jax.ShapeDtypeStruct((positions, 2 * lanes), f32),
-        name="near",
-    )(x, rows, across, down, facts)
+    near_sizes = functools.partial(near_kernel, heads, sizes)
+    near_operands = (x, rows, across, down, facts)
     operands = (
-        *priors,
-        near,
         rows,
         down,
         enter_one,
@@ -396,6 +382,20 @@
     )
     scratch_shapes = [pltpu.VMEM((sizes[0], lanes), f32), pltpu.VMEM((sizes[1], lanes), f32)]
     if order is None:
+        near = pl.pallas_call(
+            near_sizes,
+            grid=(blocks,),
+            in_specs=[
+                by_block(BLOCK, 2 * lanes),
+                by_block(BLOCK, width),
+                along(2 * high),
+                by_block(BLOCK, BLOCK),
+                fixed(6, heads),
+            ],
+            out_specs=by_block(BLOCK, 2 * lanes),
+            out_shape=jax.ShapeDtypeStruct((positions, 2 * lanes), f32),
+            name="near",
+        )(*near_operands)
         return pl.pallas_call(
             functools.partial(mixed_kernel, heads, sizes, len(priors)),
             grid=(blocks,),
@@ -414,7 +414,7 @@
             out_shape=jax.ShapeDtypeStruct((positions, 2 * lanes), bf16),
             scratch_shapes=scratch_shapes,
             name="mixed",
-        )(*operands)
+        )(*priors, near, *operands)
 
     def whole(*shape):
         return pl.BlockSpec(shape, lambda k, order: (0,) * len(shape))
@@ -434,6 +434,23 @@
             rest = (0,) * len(shape)
             return pl.BlockSpec((1, *shape), lambda k, order: (target(k, order), *rest))
 
+        near = pl.pallas_call(
+            lambda order_ref, *refs: near_sizes(*refs),
+            grid_spec=pltpu.PrefetchScalarGridSpec(
+                num_scalar_prefetch=1,
+                grid=(count,),
+                in_specs=[
+                    chosen(BLOCK, 2 * lanes),
+                    chosen(BLOCK, width),
+                    pl.BlockSpec((2 * high, BLOCK), lambda k, order, t=target: (0, t(k, order))),
+                    chosen(BLOCK, BLOCK),
+                    whole(6, heads),
+                ],
+                out_specs=pl.BlockSpec((BLOCK, 2 * lanes), lambda k, order: (k, 0)),
+            ),
+            out_shape=jax.ShapeDtypeStruct((count * BLOCK, 2 * lanes), f32),
+            name="near",
+        )(order[None], *near_operands)
         results = pl.pallas_call(
             functools.partial(projected_kernel, heads, sizes, len(priors), count),
             grid_spec=pltpu.PrefetchScalarGridSpec(
@@ -441,7 +458,7 @@
                 grid=(count,),
                 in_specs=[whole(packed_rows, lanes) for _ in priors]
                 + [
-                    chosen(BLOCK, 2 * lanes),
+                    pl.BlockSpec((BLOCK, 2 * lanes), lambda k, order: (k, 0)),
                     chosen(BLOCK, width),
                     chosen(BLOCK, BLOCK),
                     chosen_state(sizes[0], lanes),
@@ -456,7 +473,7 @@
             ),
             out_shape=[jax.ShapeDtypeStruct((BLOCK, model_width), bf16)] * count,
             name="projected",
-        )(order[None], *operands, output_matrix.reshape(2 * lanes, model_width))
+        )(order[None], *priors, near, *operands, output_matrix.reshape(2 * lanes, model_width))
         outs.update(zip(turns, results))
     return [outs[turn] for turn in range(blocks)]
 
@@ -512,10 +529,10 @@
 
 
 def expert_kernel(region, own_ref, *refs):
-    count = len(refs) - 9
+    count = (len(refs) - 7) // 2
     blocks = refs[:count]
-    keep_ref, send_ref = refs[count + 3 : count + 5]
-    gate_ref, up_ref, back_ref, arrived = refs[count + 5 :]
+    outs = refs[count + 3 : 2 * count + 3]
+    gate_ref, up_ref, back_ref, arrived = refs[2 * count + 3 :]
     fetches = [
         pltpu.make_async_copy(source, target, arrived.at[i])
         for i, (source, target) in enumerate(zip(refs[count : count + 3], (gate_ref, up_ref, back_ref)))
@@ -564,11 +581,7 @@
             result[i * region : (i + 1) * region].astype(jnp.bfloat16),
             preferred_element_type=jnp.float32,
         )
-        out_ref = (keep_ref, send_ref)[2 * i // count]
-        first = i % (count // 2) * rows
-        out_ref[first : first + rows] = (
-            spread * down[:, count + i : count + i + 1]
-        ).astype(jnp.bfloat16)
+        outs[i][...] = (spread * down[:, count + i : count + i + 1]).astype(jnp.bfloat16)
 
 
 def run_expert(blocks, own, gate_weight, up_weight, down_weight, capacity):
@@ -581,8 +594,8 @@
         in_specs=[pl.BlockSpec(memory_space=pltpu.SMEM)]
         + [vmem] * len(blocks)
         + [pl.BlockSpec(memory_space=pl.ANY)] * 3,
-        out_specs=[vmem] * 2,
-        out_shape=[jax.ShapeDtypeStruct((len(blocks) // 2 * rows, width), jnp.bfloat16)] * 2,
+        out_specs=[vmem] * len(blocks),
+        out_shape=[jax.ShapeDtypeStruct((rows, width), jnp.bfloat16)] * len(blocks),
         scratch_shapes=[
             pltpu.VMEM((width, hidden), jnp.bfloat16),
             pltpu.VMEM((width, hidden), jnp.bfloat16),
@@ -670,14 +683,9 @@
 
 
 def near_added(keep, back):
-    rows, width = keep.shape
-    half = pl.BlockSpec((rows // 2, width), lambda k: (0, 0))
     return pl.pallas_call(
         near_kernel_sum,
-        grid=(1,),
-        in_specs=[half, half],
-        out_specs=half,
-        out_shape=jax.ShapeDtypeStruct((rows // 2, width), jnp.bfloat16),
+        out_shape=jax.ShapeDtypeStruct(keep.shape, jnp.bfloat16),
         name="near_sum",
     )(keep, back)
 
@@ -708,15 +716,15 @@
     for turns in ((0, 1), (2,), (3,)):
         kept = [b for turn in turns for b in (blocks[turn], far[turn])]
         sent = [b for turn in turns for b in (near_other[turn], far_other[turn])]
-        keep, send = run_expert(kept + sent, *experts)
-        back = swapped(send, 1)
-        fenced = lax.optimization_barrier((keep, back))
+        results = run_expert(kept + sent, *experts)
         for i, turn in enumerate(turns):
-            here = slice(2 * i * rows, (2 * i + 1) * rows)
-            beyond = slice((2 * i + 1) * rows, 2 * (i + 1) * rows)
-            near.append((fenced[0][here], fenced[1][here]))
-            crossed.append(swapped(added(keep[beyond], back[beyond]), 2))
-    near_last = near_added(keep, back)
+            keep_near, keep_far = results[2 * i : 2 * i + 2]
+            send_near, send_far = results[len(kept) + 2 * i : len(kept) + 2 * i + 2]
+            back_far = swapped(send_far, 1)
+            back_near = swapped(send_near, 1)
+            near.append((keep_near, back_near))
+            crossed.append(swapped(added(keep_far, back_far), 2))
+    near_last = near_added(*near[3])
     parts = [None]
     for turn in (1, 2):
         parts.append(added(*near[turn], crossed[turn]))

time: 252 us -> 265 us (1.052)
  waiting for transfers between devices: 75.3 us -> 128 us
  starting transfers between devices: 88.5 us -> 52.6 us
  other arithmetic: 12.1 us -> 8.51 us
    ppermute x2, starting transfers between devices: 26.4 us -> 0.14 us  [line_sum(): pair = lax.ppermute(added(parts[1], middle), 'tp', SWAPS)]
    ppermute x19 -> x24, waiting for transfers between devices: 34.6 us -> 57.5 us  [swapped(): lax.ppermute(array, 'sp', [(i, i ^ bit) for i in range(lax.axis_size('sp'...]
    ppermute x2, waiting for transfers between devices: 0.01 us -> 17.7 us  [line_sum(): ends = lax.ppermute(parts[2], 'tp', ENDS)]
    ppermute x19 -> x24, starting transfers between devices: 25.8 us -> 15.2 us  [swapped(): lax.ppermute(array, 'sp', [(i, i ^ bit) for i in range(lax.axis_size('sp'...]
    ppermute x1, waiting for transfers between devices: 6.44 us -> 12.3 us  [dense_experts(): from_pair = lax.ppermute(normed, 'tp', SWAPS)]
    ppermute x1, waiting for transfers between devices: 6.71 us -> 10.8 us  [dense_experts(): outer_two = lax.ppermute(second, 'tp', OUTWARD)]
    add x8 -> x9, other arithmetic: 9.47 us -> 5.51 us  [added(): return block + received[0]]
    pallas_call x2 -> x3, Pallas kernels: 6.78 us -> 8.18 us  [the longest x2 6 us: mixed_rows(): pl.pallas_call(lambda order_ref, *refs: near_sizes(*refs), grid_spec=pltp...]
  transfers between devices with their start and end apart: 37 -> 42, of which waited for: 11 -> 15; matrix products, arithmetic and copies ran while one was open for 5% -> 4% of each run, Pallas kernels for 19% -> 18%
where the time goes in v2:
time: 265 us; the launch traced here: 264 us
  waiting for transfers between devices  128 us (48%)
  Pallas kernels  68.4 us (26%)
  starting transfers between devices  52.6 us (20%)
  other arithmetic  8.51 us (3%)
  local copies, waits for them, and re-layouts  6.39 us (2%)
    ppermute x24, waiting for transfers between devices, swapped(): lax.ppermute(array, 'sp', [(i, i ^ bit) for i in range(lax.axis_size('sp'...  57.5 us
    pallas_call x3, Pallas kernels, run_expert(): pl.pallas_call(functools.partial(expert_kernel, region), in_specs=[pl.Blo...  33.6 us
    ppermute x2, waiting for transfers between devices, line_sum(): ends = lax.ppermute(parts[2], 'tp', ENDS)  17.7 us
    ppermute x2, waiting for transfers between devices, line_sum(): pair = lax.ppermute(added(parts[1], middle), 'tp', SWAPS)  17.6 us
    ppermute x24, starting transfers between devices, swapped(): lax.ppermute(array, 'sp', [(i, i ^ bit) for i in range(lax.axis_size('sp'...  15.2 us
    pallas_call x2, Pallas kernels, mixed_rows(): pl.pallas_call(functools.partial(projected_kernel, heads, sizes, len(prio...  13.3 us
    ppermute x1, waiting for transfers between devices, dense_experts(): from_pair = lax.ppermute(normed, 'tp', SWAPS)  12.3 us
    ppermute x4, starting transfers between devices, passed_along(): return lax.ppermute(shard, axis, pairs)  11.8 us
  transfers between devices with their start and end apart: 42, of which 15 were waited for; matrix products, arithmetic and copies ran while one was open for 4% of the time, Pallas kernels for 18%

profile of v2, /device:TPU:0, one launch (start us, length us, event | category | flops | bytes accessed | tf_op | source)
XLA Modules:
  0.0 264.3 jit_solution(400754903512529843)
XLA Ops:
  5.7 7.0 %states.1 = (bf16[512,512]{1,0:T(8,128)(2,1)}, bf16[512,384]{1,0:T(8,128)(2,1)}, f32[16,512]{1,0:T(8,128)}, f32[512,128]{1,0:T(8,128)}, f32[4,64,256]{2,1,0:T(8,...) custom-call(bf16[512,2,256]{2,1,0:T(2,128)(2,1)} %values_ref.1, ...), custom_call_target="tpu_custom_call" | custom-call | tf_op jit(solution)/shard_map/states/pallas_call | solution.py:321
  12.8 4.5 %collective-permute-start.1 = (bf16[208,256]{1,0:T(8,128)(2,1)}, bf16[208,256]{1,0:T(8,128)(2,1)S(1)}, u32[]{:S(2)}, u32[]{:S(2)}) collective-permute-start(bf16[208,256]{1,0:T(8,128)(2,1)} %get-tuple-element.35), channel_id=1, source_target_pairs={{0,4},{4,8},{8,12},{1,5},{5,9},{9,13},{2,6},{6,10},{10,14},{3,7},{... | collective-permute-start | bytes 319496 | tf_op jit(solution)/shard_map/ppermute | solution.py:23
  17.3 3.6 %collective-permute-start.2 = (bf16[208,256]{1,0:T(8,128)(2,1)}, bf16[208,256]{1,0:T(8,128)(2,1)S(1)}, u32[]{:S(2)}, u32[]{:S(2)}) collective-permute-start(bf16[208,256]{1,0:T(8,128)(2,1)} %get-tuple-element.35), channel_id=1, source_target_pairs={{0,8},{4,12},{1,9},{5,13},{2,10},{6,14},{3,11},{7,15},{16,24},{20,... | collective-permute-start | bytes 319496 | tf_op jit(solution)/shard_map/ppermute | solution.py:23
  26.0 6.6 %projected.3 = (bf16[128,2048]{1,0:T(8,128)(2,1)}, bf16[128,2048]{1,0:T(8,128)(2,1)}) custom-call(s32[1]{0:T(128)} %bitcast.order_ref, bf16[208,256]{1,0:T(8,128)(2,1)} %copy-done.20, bf16[208,256]{1,0:T(8,128)(2,1)} %copy-done.21, bf16[208,256]{1,0:T(8,128)(2,1)} %copy-done.22, f32[256,512]{1,0:T(8,128)} %near.3.refs_3_, ...), custom_call_target="tpu_custom_call" | custom-call | tf_op jit(solution)/shard_map/projected/pallas_call | solution.py:454
  33.4 6.3 %collective-permute-start.7 = (bf16[128,2048]{1,0:T(8,128)(2,1)}, bf16[128,2048]{1,0:T(8,128)(2,1)S(1)}, u32[]{:S(2)}, u32[]{:S(2)}) collective-permute-start(bf16[128,2048]{1,0:T(8,128)(2,1)} %get-tuple-element.46), channel_id=1, source_target_pairs={{0,1},{3,2},{4,5},{7,6},{8,9},{11,10},{12,13},{15,14},{16,17},{19,... | collective-permute-start | bytes 1572872 | tf_op jit(solution)/shard_map/ppermute | solution.py:666
  46.1 6.6 %projected.2 = (bf16[128,2048]{1,0:T(8,128)(2,1)}, bf16[128,2048]{1,0:T(8,128)(2,1)}) custom-call(s32[1]{0:T(128)} %bitcast.order_ref, bf16[208,256]{1,0:T(8,128)(2,1)} %copy-done.20, bf16[208,256]{1,0:T(8,128)(2,1)} %copy-done.21, bf16[208,256]{1,0:T(8,128)(2,1)} %copy-done.22, f32[256,512]{1,0:T(8,128)} %near.2.refs_3_, ...), custom_call_target="tpu_custom_call" | custom-call | tf_op jit(solution)/shard_map/projected/pallas_call | solution.py:454
  55.7 9.6 %collective-permute-done.4.one_ref = bf16[128,2048]{1,0:T(8,128)(2,1)S(1)} collective-permute-done((bf16[128,2048]{1,0:T(8,128)(2,1)}, bf16[128,2048]{1,0:T(8,128)(2,1)S(1)}, u32[]{:S(2)}, u32[]{:S(2)}) %collective-permute-start.4) | collective-permute-done | bytes 524320 | tf_op jit(solution)/shard_map/ppermute | solution.py:664
  65.4 8.8 %collective-permute-done.6.two_ref = bf16[128,2048]{1,0:T(8,128)(2,1)S(1)} collective-permute-done((bf16[128,2048]{1,0:T(8,128)(2,1)S(1)}, bf16[128,2048]{1,0:T(8,128)(2,1)S(1)}, u32[]{:S(2)}, u32[]{:S(2)}) %collective-permute-start.6) | collective-permute-done | bytes 524320 | tf_op jit(solution)/shard_map/ppermute | solution.py:667
  81.1 12.3 %collective-permute-done.10.refs_2_ = bf16[128,2176]{1,0:T(8,128)(2,1)} collective-permute-done((bf16[128,2176]{1,0:T(8,128)(2,1)}, bf16[128,2176]{1,0:T(8,128)(2,1)}, u32[]{:S(2)}, u32[]{:S(2)}) %collective-permute-start.10) | collective-permute-done | bytes 557088 | tf_op jit(solution)/shard_map/ppermute | solution.py:701
  94.1 11.6 %collective-permute-done.19.refs_0_ = bf16[128,2176]{1,0:T(8,128)(2,1)S(1)} collective-permute-done((bf16[128,2176]{1,0:T(8,128)(2,1)}, bf16[128,2176]{1,0:T(8,128)(2,1)S(1)}, u32[]{:S(2)}, u32[]{:S(2)}) %collective-permute-start.19) | collective-permute-done | bytes 557088 | tf_op jit(solution)/shard_map/ppermute | solution.py:702
  110.2 10.8 %collective-permute-done.31 = bf16[128,2176]{1,0:T(8,128)(2,1)S(1)} collective-permute-done((bf16[128,2176]{1,0:T(8,128)(2,1)S(1)}, bf16[128,2176]{1,0:T(8,128)(2,1)S(1)}, u32[]{:S(2)}, u32[]{:S(2)}) %collective-permute-start.31) | collective-permute-done | bytes 557088 | tf_op jit(solution)/shard_map/ppermute | solution.py:704
  124.3 11.4 %collective-permute-done.20.refs_1_ = bf16[128,2176]{1,0:T(8,128)(2,1)S(1)} collective-permute-done((bf16[128,2176]{1,0:T(8,128)(2,1)S(1)}, bf16[128,2176]{1,0:T(8,128)(2,1)S(1)}, u32[]{:S(2)}, u32[]{:S(2)}) %collective-permute-start.20) | collective-permute-done | bytes 557088 | tf_op jit(solution)/shard_map/ppermute | solution.py:528
  136.3 11.4 %collective-permute-done.32.refs_1_ = bf16[128,2176]{1,0:T(8,128)(2,1)S(1)} collective-permute-done((bf16[128,2176]{1,0:T(8,128)(2,1)S(1)}, bf16[128,2176]{1,0:T(8,128)(2,1)S(1)}, u32[]{:S(2)}, u32[]{:S(2)}) %collective-permute-start.32) | collective-permute-done | bytes 557088 | tf_op jit(solution)/shard_map/ppermute | solution.py:528
  147.7 10.4 %collective-permute-done.11.refs_3_ = bf16[128,2176]{1,0:T(8,128)(2,1)} collective-permute-done((bf16[128,2176]{1,0:T(8,128)(2,1)}, bf16[128,2176]{1,0:T(8,128)(2,1)}, u32[]{:S(2)}, u32[]{:S(2)}) %collective-permute-start.11) | collective-permute-done | bytes 557088 | tf_op jit(solution)/shard_map/ppermute | solution.py:528
  159.2 9.4 %expert.4 = (bf16[128,2048]{1,0:T(8,128)(2,1)}, bf16[128,2048]{1,0:T(8,128)(2,1)}, bf16[128,2048]{1,0:T(8,128)(2,1)}, bf16[128,2048]{1,0:T(8,128)(2,1)}) custom-call(s32[1]{0:T(128)} %bitcast.5.own_ref, bf16[128,2176]{1,0:T(8,128)(2,1)} %copy-done.1, bf16[128,2176]{1,0:T(8,128)(2,1)} %copy-done.3, bf16[128,2176]{1,0:T(8,128)(2,1)} %copy-done.5, ...), custom_call_target="tpu_custom_call" | custom-call | flops 3623878656 | bytes 12582912 | tf_op jit(solution)/shard_map/expert/pallas_call | solution.py:592
  169.0 9.5 %expert.5 = (bf16[128,2048]{1,0:T(8,128)(2,1)}, bf16[128,2048]{1,0:T(8,128)(2,1)}, bf16[128,2048]{1,0:T(8,128)(2,1)}, bf16[128,2048]{1,0:T(8,128)(2,1)}) custom-call(s32[1]{0:T(128)} %bitcast.5.own_ref, bf16[128,2176]{1,0:T(8,128)(2,1)} %copy-done, bf16[128,2176]{1,0:T(8,128)(2,1)} %copy-done.2, bf16[128,2176]{1,0:T(8,128)(2,1)} %copy-done.4, ...), custom_call_target="tpu_custom_call" | custom-call | flops 3623878656 | bytes 12582912 | tf_op jit(solution)/shard_map/expert/pallas_call | solution.py:592
  178.8 14.7 %expert.3 = (bf16[128,2048]{1,0:T(8,128)(2,1)}, bf16[128,2048]{1,0:T(8,128)(2,1)}, bf16[128,2048]{1,0:T(8,128)(2,1)}, bf16[128,2048]{1,0:T(8,128)(2,1)}, bf16[12...) custom-call(s32[1]{0:T(128)} %bitcast.5.own_ref, ...), custom_call_target="tpu_custom_call" | custom-call | flops 7247757312 | bytes 12582912 | tf_op jit(solution)/shard_map/expert/pallas_call | solution.py:592
  202.2 8.1 %collective-permute-done.37 = bf16[128,2048]{1,0:T(8,128)(2,1)} collective-permute-done((bf16[128,2048]{1,0:T(8,128)(2,1)}, bf16[128,2048]{1,0:T(8,128)(2,1)}, u32[]{:S(2)}, u32[]{:S(2)}) %collective-permute-start.37) | collective-permute-done | bytes 524320 | tf_op jit(solution)/shard_map/ppermute | solution.py:528
  214.2 7.2 %collective-permute-done.25 = bf16[128,2048]{1,0:T(8,128)(2,1)} collective-permute-done((bf16[128,2048]{1,0:T(8,128)(2,1)S(1)}, bf16[128,2048]{1,0:T(8,128)(2,1)}, u32[]{:S(2)}, u32[]{:S(2)}) %collective-permute-start.25) | collective-permute-done | bytes 524320 | tf_op jit(solution)/shard_map/ppermute | solution.py:528
  221.5 4.3 %collective-permute-start.40 = (bf16[128,2048]{1,0:T(8,128)(2,1)S(1)}, bf16[128,2048]{1,0:T(8,128)(2,1)S(1)}, u32[]{:S(2)}, u32[]{:S(2)}) collective-permute-start(bf16[128,2048]{1,0:T(8,128)(2,1)S(1)} %add.51), channel_id=1, source_target_pairs={{0,1},{3,2},{4,5},{7,6},{8,9},{11,10},{12,13},{15,14},{16,17},{19,... | collective-permute-start | bytes 1572872 | tf_op jit(solution)/shard_map/ppermute | solution.py:666
  232.6 3.4 %collective-permute-start.26 = (bf16[128,2048]{1,0:T(8,128)(2,1)S(1)}, bf16[128,2048]{1,0:T(8,128)(2,1)S(1)}, u32[]{:S(2)}, u32[]{:S(2)}) collective-permute-start(bf16[128,2048]{1,0:T(8,128)(2,1)S(1)} %add_convert_fusion.1), channel_id=1, source_target_pairs={{0,3},{3,0},{4,7},{7,4},{8,11},{11,8},{12,15},{15,12},{16,19},{19,... | collective-permute-start | bytes 1572872 | tf_op jit(solution)/shard_map/ppermute | solution.py:664
  237.6 5.5 %collective-permute-done.18.refs_2_ = bf16[128,2048]{1,0:T(8,128)(2,1)S(1)} collective-permute-done((bf16[128,2048]{1,0:T(8,128)(2,1)S(1)}, bf16[128,2048]{1,0:T(8,128)(2,1)S(1)}, u32[]{:S(2)}, u32[]{:S(2)}) %collective-permute-start.18) | collective-permute-done | bytes 524320 | tf_op jit(solution)/shard_map/ppermute | solution.py:528
  243.1 8.0 %collective-permute-done.26.refs_3_ = bf16[128,2048]{1,0:T(8,128)(2,1)S(1)} collective-permute-done((bf16[128,2048]{1,0:T(8,128)(2,1)S(1)}, bf16[128,2048]{1,0:T(8,128)(2,1)S(1)}, u32[]{:S(2)}, u32[]{:S(2)}) %collective-permute-start.26) | collective-permute-done | bytes 524320 | tf_op jit(solution)/shard_map/ppermute | solution.py:664
  251.2 8.8 %collective-permute-done.39.refs_4_ = bf16[128,2048]{1,0:T(8,128)(2,1)S(1)} collective-permute-done((bf16[128,2048]{1,0:T(8,128)(2,1)S(1)}, bf16[128,2048]{1,0:T(8,128)(2,1)S(1)}, u32[]{:S(2)}, u32[]{:S(2)}) %collective-permute-start.39) | collective-permute-done | bytes 524320 | tf_op jit(solution)/shard_map/ppermute | solution.py:667
  (146 shorter events, 63.6 us)
Async XLA Ops:
  32.6 20.2 %collective-permute-start.5 = (bf16[128,2048]{1,0:T(8,128)(2,1)}, bf16[128,2048]{1,0:T(8,128)(2,1)S(1)}, u32[]{:S(2)}, u32[]{:S(2)}) collective-permute-start(bf16[128,2048]{1,0:T(8,128)(2,1)} %get-tuple-element.46), channel_id=1, source_target_pairs={{1,2},{2,1},{5,6},{6,5},{9,10},{10,9},{13,14},{14,13},{17,18},{18,... | collective-permute-start | bytes 1572872 | tf_op jit(solution)/shard_map/ppermute | solution.py:665
  33.4 20.6 %collective-permute-start.7 = (bf16[128,2048]{1,0:T(8,128)(2,1)}, bf16[128,2048]{1,0:T(8,128)(2,1)S(1)}, u32[]{:S(2)}, u32[]{:S(2)}) collective-permute-start(bf16[128,2048]{1,0:T(8,128)(2,1)} %get-tuple-element.46), channel_id=1, source_target_pairs={{0,1},{3,2},{4,5},{7,6},{8,9},{11,10},{12,13},{15,14},{16,17},{19,... | collective-permute-start | bytes 1572872 | tf_op jit(solution)/shard_map/ppermute | solution.py:666
  42.7 22.6 %collective-permute-start.4 = (bf16[128,2048]{1,0:T(8,128)(2,1)}, bf16[128,2048]{1,0:T(8,128)(2,1)S(1)}, u32[]{:S(2)}, u32[]{:S(2)}) collective-permute-start(bf16[128,2048]{1,0:T(8,128)(2,1)} %get-tuple-element.44), channel_id=1, source_target_pairs={{0,3},{3,0},{4,7},{7,4},{8,11},{11,8},{12,15},{15,12},{16,19},{19,... | collective-permute-start | bytes 1572872 | tf_op jit(solution)/shard_map/ppermute | solution.py:664
  54.0 20.2 %collective-permute-start.6 = (bf16[128,2048]{1,0:T(8,128)(2,1)S(1)}, bf16[128,2048]{1,0:T(8,128)(2,1)S(1)}, u32[]{:S(2)}, u32[]{:S(2)}) collective-permute-start(bf16[128,2048]{1,0:T(8,128)(2,1)S(1)} %add.41), channel_id=1, source_target_pairs={{0,1},{1,0},{2,3},{3,2},{4,5},{5,4},{6,7},{7,6},{8,9},{9,8},{10,11... | collective-permute-start | bytes 1572872 | tf_op jit(solution)/shard_map/ppermute | solution.py:667
  78.9 26.8 %collective-permute-start.19 = (bf16[128,2176]{1,0:T(8,128)(2,1)}, bf16[128,2176]{1,0:T(8,128)(2,1)S(1)}, u32[]{:S(2)}, u32[]{:S(2)}) collective-permute-start(bf16[128,2176]{1,0:T(8,128)(2,1)} %get-tuple-element.48.refs_0_), channel_id=1, source_target_pairs={{1,2},{2,1},{0,3},{3,0},{5,6},{6,5},{4,7},{7,4},{9,10},{10,9},{8,1... | collective-permute-start | bytes 1671176 | tf_op jit(solution)/shard_map/ppermute | solution.py:702
  107.2 28.6 %collective-permute-start.9 = (bf16[128,2176]{1,0:T(8,128)(2,1)}, bf16[128,2176]{1,0:T(8,128)(2,1)S(1)}, u32[]{:S(2)}, u32[]{:S(2)}) collective-permute-start(bf16[128,2176]{1,0:T(8,128)(2,1)} %get-tuple-element.48.refs_0_), channel_id=1, source_target_pairs={{0,8},{4,12},{8,0},{12,4},{1,9},{5,13},{9,1},{13,5},{2,10},{6,14},... | collective-permute-start | bytes 1671176 | tf_op jit(solution)/shard_map/ppermute | solution.py:528
  110.1 25.6 %collective-permute-start.20 = (bf16[128,2176]{1,0:T(8,128)(2,1)S(1)}, bf16[128,2176]{1,0:T(8,128)(2,1)S(1)}, u32[]{:S(2)}, u32[]{:S(2)}) collective-permute-start(bf16[128,2176]{1,0:T(8,128)(2,1)S(1)} %collective-permute-done.19.refs_0_), channel_id=1, source_target_pairs={{0,8},{4,12},{8,0},{12,4},{1,9},{5,13},{9,1},{13,5},{2,10},{6,14},... | collective-permute-start | bytes 1671176 | tf_op jit(solution)/shard_map/ppermute | solution.py:528
  121.1 26.6 %collective-permute-start.32 = (bf16[128,2176]{1,0:T(8,128)(2,1)S(1)}, bf16[128,2176]{1,0:T(8,128)(2,1)S(1)}, u32[]{:S(2)}, u32[]{:S(2)}) collective-permute-start(bf16[128,2176]{1,0:T(8,128)(2,1)S(1)} %broadcast_select_fusion.refs_0_), channel_id=1, source_target_pairs={{0,8},{4,12},{8,0},{12,4},{1,9},{5,13},{9,1},{13,5},{2,10},{6,14},... | collective-permute-start | bytes 1671176 | tf_op jit(solution)/shard_map/ppermute | solution.py:528
  124.3 33.9 %collective-permute-start.11 = (bf16[128,2176]{1,0:T(8,128)(2,1)}, bf16[128,2176]{1,0:T(8,128)(2,1)}, u32[]{:S(2)}, u32[]{:S(2)}) collective-permute-start(bf16[128,2176]{1,0:T(8,128)(2,1)} %collective-permute-done.10.refs_2_), channel_id=1, source_target_pairs={{0,8},{4,12},{8,0},{12,4},{1,9},{5,13},{9,1},{13,5},{2,10},{6,14},... | collective-permute-start | bytes 1671176 | tf_op jit(solution)/shard_map/ppermute | solution.py:528
  124.3 33.8 %collective-permute-start.21 = (bf16[128,2176]{1,0:T(8,128)(2,1)S(1)}, bf16[128,2176]{1,0:T(8,128)(2,1)S(1)}, u32[]{:S(2)}, u32[]{:S(2)}) collective-permute-start(bf16[128,2176]{1,0:T(8,128)(2,1)S(1)} %collective-permute-done.19.refs_0_), channel_id=1, source_target_pairs={{0,4},{4,0},{8,12},{12,8},{1,5},{5,1},{9,13},{13,9},{2,6},{6,2},{1... | collective-permute-start | bytes 1671176 | tf_op jit(solution)/shard_map/ppermute | solution.py:528
  135.8 22.9 %collective-permute-start.22 = (bf16[128,2176]{1,0:T(8,128)(2,1)S(1)}, bf16[128,2176]{1,0:T(8,128)(2,1)}, u32[]{:S(2)}, u32[]{:S(2)}) collective-permute-start(bf16[128,2176]{1,0:T(8,128)(2,1)S(1)} %collective-permute-done.20.refs_1_), channel_id=1, source_target_pairs={{0,4},{4,0},{8,12},{12,8},{1,5},{5,1},{9,13},{13,9},{2,6},{6,2},{1... | collective-permute-start | bytes 1671176 | tf_op jit(solution)/shard_map/ppermute | solution.py:528
  135.8 23.0 %collective-permute-start.33 = (bf16[128,2176]{1,0:T(8,128)(2,1)S(1)}, bf16[128,2176]{1,0:T(8,128)(2,1)S(1)}, u32[]{:S(2)}, u32[]{:S(2)}) collective-permute-start(bf16[128,2176]{1,0:T(8,128)(2,1)S(1)} %broadcast_select_fusion.refs_0_), channel_id=1, source_target_pairs={{0,4},{4,0},{8,12},{12,8},{1,5},{5,1},{9,13},{13,9},{2,6},{6,2},{1... | collective-permute-start | bytes 1671176 | tf_op jit(solution)/shard_map/ppermute | solution.py:528
  147.7 20.9 %collective-permute-start.34 = (bf16[128,2176]{1,0:T(8,128)(2,1)S(1)}, bf16[128,2176]{1,0:T(8,128)(2,1)}, u32[]{:S(2)}, u32[]{:S(2)}) collective-permute-start(bf16[128,2176]{1,0:T(8,128)(2,1)S(1)} %collective-permute-done.32.refs_1_), channel_id=1, source_target_pairs={{0,4},{4,0},{8,12},{12,8},{1,5},{5,1},{9,13},{13,9},{2,6},{6,2},{1... | collective-permute-start | bytes 1671176 | tf_op jit(solution)/shard_map/ppermute | solution.py:528
  158.2 20.3 %collective-permute-start.12 = (bf16[128,2176]{1,0:T(8,128)(2,1)}, bf16[128,2176]{1,0:T(8,128)(2,1)}, u32[]{:S(2)}, u32[]{:S(2)}) collective-permute-start(bf16[128,2176]{1,0:T(8,128)(2,1)} %get-tuple-element.48.refs_0_), channel_id=1, source_target_pairs={{0,4},{4,0},{8,12},{12,8},{1,5},{5,1},{9,13},{13,9},{2,6},{6,2},{1... | collective-permute-start | bytes 1671176 | tf_op jit(solution)/shard_map/ppermute | solution.py:528
  158.2 20.7 %collective-permute-start.14 = (bf16[128,2176]{1,0:T(8,128)(2,1)}, bf16[128,2176]{1,0:T(8,128)(2,1)}, u32[]{:S(2)}, u32[]{:S(2)}) collective-permute-start(bf16[128,2176]{1,0:T(8,128)(2,1)} %collective-permute-done.10.refs_2_), channel_id=1, source_target_pairs={{0,4},{4,0},{8,12},{12,8},{1,5},{5,1},{9,13},{13,9},{2,6},{6,2},{1... | collective-permute-start | bytes 1671176 | tf_op jit(solution)/shard_map/ppermute | solution.py:528
  158.7 20.1 %collective-permute-start.13 = (bf16[128,2176]{1,0:T(8,128)(2,1)}, bf16[128,2176]{1,0:T(8,128)(2,1)}, u32[]{:S(2)}, u32[]{:S(2)}) collective-permute-start(bf16[128,2176]{1,0:T(8,128)(2,1)} %copy-done.25), channel_id=1, source_target_pairs={{0,4},{4,0},{8,12},{12,8},{1,5},{5,1},{9,13},{13,9},{2,6},{6,2},{1... | collective-permute-start | bytes 1671176 | tf_op jit(solution)/shard_map/ppermute | solution.py:528
  168.7 28.2 %collective-permute-start.24 = (bf16[128,2048]{1,0:T(8,128)(2,1)}, bf16[128,2048]{1,0:T(8,128)(2,1)S(1)}, u32[]{:S(2)}, u32[]{:S(2)}) collective-permute-start(bf16[128,2048]{1,0:T(8,128)(2,1)} %get-tuple-element.56), channel_id=1, source_target_pairs={{0,4},{4,0},{8,12},{12,8},{1,5},{5,1},{9,13},{13,9},{2,6},{6,2},{1... | collective-permute-start | bytes 1572872 | tf_op jit(solution)/shard_map/ppermute | solution.py:528
  197.5 24.0 %collective-permute-start.25 = (bf16[128,2048]{1,0:T(8,128)(2,1)S(1)}, bf16[128,2048]{1,0:T(8,128)(2,1)}, u32[]{:S(2)}, u32[]{:S(2)}) collective-permute-start(bf16[128,2048]{1,0:T(8,128)(2,1)S(1)} %add.45), channel_id=1, source_target_pairs={{0,8},{4,12},{8,0},{12,4},{1,9},{5,13},{9,1},{13,5},{2,10},{6,14},... | collective-permute-start | bytes 1572872 | tf_op jit(solution)/shard_map/ppermute | solution.py:528
  200.0 27.4 %collective-permute-start.27 = (bf16[128,2048]{1,0:T(8,128)(2,1)}, bf16[128,2048]{1,0:T(8,128)(2,1)S(1)}, u32[]{:S(2)}, u32[]{:S(2)}) collective-permute-start(bf16[128,2048]{1,0:T(8,128)(2,1)} %get-tuple-element.58), channel_id=1, source_target_pairs={{0,4},{4,0},{8,12},{12,8},{1,5},{5,1},{9,13},{13,9},{2,6},{6,2},{1... | collective-permute-start | bytes 1572872 | tf_op jit(solution)/shard_map/ppermute | solution.py:528
  210.2 22.4 %collective-permute-start.29 = (bf16[128,2048]{1,0:T(8,128)(2,1)S(1)}, bf16[128,2048]{1,0:T(8,128)(2,1)S(1)}, u32[]{:S(2)}, u32[]{:S(2)}) collective-permute-start(bf16[128,2048]{1,0:T(8,128)(2,1)S(1)} %add.48), channel_id=1, source_target_pairs={{0,8},{4,12},{8,0},{12,4},{1,9},{5,13},{9,1},{13,5},{2,10},{6,14},... | collective-permute-start | bytes 1572872 | tf_op jit(solution)/shard_map/ppermute | solution.py:528
  213.3 22.7 %collective-permute-start.38 = (bf16[128,2048]{1,0:T(8,128)(2,1)S(1)}, bf16[128,2048]{1,0:T(8,128)(2,1)S(1)}, u32[]{:S(2)}, u32[]{:S(2)}) collective-permute-start(bf16[128,2048]{1,0:T(8,128)(2,1)S(1)} %add.51), channel_id=1, source_target_pairs={{1,2},{2,1},{5,6},{6,5},{9,10},{10,9},{13,14},{14,13},{17,18},{18,... | collective-permute-start | bytes 1572872 | tf_op jit(solution)/shard_map/ppermute | solution.py:665
  214.2 23.5 %collective-permute-start.16 = (bf16[128,2048]{1,0:T(8,128)(2,1)}, bf16[128,2048]{1,0:T(8,128)(2,1)S(1)}, u32[]{:S(2)}, u32[]{:S(2)}) collective-permute-start(bf16[128,2048]{1,0:T(8,128)(2,1)} %get-tuple-element.50), channel_id=1, source_target_pairs={{0,4},{4,0},{8,12},{12,8},{1,5},{5,1},{9,13},{13,9},{2,6},{6,2},{1... | collective-permute-start | bytes 1572872 | tf_op jit(solution)/shard_map/ppermute | solution.py:528
  236.4 23.6 %collective-permute-start.39 = (bf16[128,2048]{1,0:T(8,128)(2,1)S(1)}, bf16[128,2048]{1,0:T(8,128)(2,1)S(1)}, u32[]{:S(2)}, u32[]{:S(2)}) collective-permute-start(bf16[128,2048]{1,0:T(8,128)(2,1)S(1)} %fusion), channel_id=1, source_target_pairs={{0,1},{1,0},{2,3},{3,2},{4,5},{5,4},{6,7},{7,6},{8,9},{9,8},{10,11... | collective-permute-start | bytes 1572872 | tf_op jit(solution)/shard_map/ppermute | solution.py:667
  236.9 23.1 %collective-permute-start.41 = (bf16[128,2048]{1,0:T(8,128)(2,1)S(1)}, bf16[128,2048]{1,0:T(8,128)(2,1)S(1)}, u32[]{:S(2)}, u32[]{:S(2)}) collective-permute-start(bf16[128,2048]{1,0:T(8,128)(2,1)S(1)} %add.53), channel_id=1, source_target_pairs={{1,2},{2,1},{5,6},{6,5},{9,10},{10,9},{13,14},{14,13},{17,18},{18,... | collective-permute-start | bytes 1572872 | tf_op jit(solution)/shard_map/ppermute | solution.py:668
  (45 other events, 610.2 us)

commit v3 on v2

--- a/solution.py
+++ b/solution.py
@@ -537,8 +537,8 @@
         pltpu.make_async_copy(source, target, arrived.at[i])
         for i, (source, target) in enumerate(zip(refs[count : count + 3], (gate_ref, up_ref, back_ref)))
     ]
-    for fetch in fetches:
-        fetch.start()
+    fetches[0].start()
+    fetches[1].start()
     width = gate_ref.shape[0]
     rows = blocks[0].shape[0]
     own = own_ref[0].astype(jnp.float32)
@@ -567,6 +567,7 @@
         [slot[0:count]] + weights + [jnp.zeros((rows - 2 * count, rows), jnp.float32)], axis=0
     ).T
     fetches[0].wait()
+    fetches[2].start()
     gate = jnp.dot(taken, gate_ref[...], preferred_element_type=jnp.float32)
     fetches[1].wait()
     up = jnp.dot(taken, up_ref[...], preferred_element_type=jnp.float32)

time: 265 us -> 265 us (level)
  no operation moved by 1% of the time
where the time goes in v3:
time: 265 us; the launch traced here: 264 us
  waiting for transfers between devices  128 us (48%)
  Pallas kernels  68.4 us (26%)
  starting transfers between devices  52.6 us (20%)
  other arithmetic  8.51 us (3%)
  local copies, waits for them, and re-layouts  6.39 us (2%)
    ppermute x24, waiting for transfers between devices, swapped(): lax.ppermute(array, 'sp', [(i, i ^ bit) for i in range(lax.axis_size('sp'...  57.5 us
    pallas_call x3, Pallas kernels, run_expert(): pl.pallas_call(functools.partial(expert_kernel, region), in_specs=[pl.Blo...  33.6 us
    ppermute x2, waiting for transfers between devices, line_sum(): ends = lax.ppermute(parts[2], 'tp', ENDS)  17.7 us
    ppermute x2, waiting for transfers between devices, line_sum(): pair = lax.ppermute(added(parts[1], middle), 'tp', SWAPS)  17.6 us
    ppermute x24, starting transfers between devices, swapped(): lax.ppermute(array, 'sp', [(i, i ^ bit) for i in range(lax.axis_size('sp'...  15.2 us
    pallas_call x2, Pallas kernels, mixed_rows(): pl.pallas_call(functools.partial(projected_kernel, heads, sizes, len(prio...  13.3 us
    ppermute x1, waiting for transfers between devices, dense_experts(): from_pair = lax.ppermute(normed, 'tp', SWAPS)  12.3 us
    ppermute x4, starting transfers between devices, passed_along(): return lax.ppermute(shard, axis, pairs)  11.8 us
  transfers between devices with their start and end apart: 42, of which 15 were waited for; matrix products, arithmetic and copies ran while one was open for 4% of the time, Pallas kernels for 18%

profile of v3, /device:TPU:0, one launch (start us, length us, event | category | flops | bytes accessed | tf_op | source)
XLA Modules:
  0.0 264.3 jit_solution(9805772678287057858)
XLA Ops:
  5.7 7.0 %states.1 = (bf16[512,512]{1,0:T(8,128)(2,1)}, bf16[512,384]{1,0:T(8,128)(2,1)}, f32[16,512]{1,0:T(8,128)}, f32[512,128]{1,0:T(8,128)}, f32[4,64,256]{2,1,0:T(8,...) custom-call(bf16[512,2,256]{2,1,0:T(2,128)(2,1)} %values_ref.1, ...), custom_call_target="tpu_custom_call" | custom-call | tf_op jit(solution)/shard_map/states/pallas_call | solution.py:321
  12.8 4.5 %collective-permute-start.1 = (bf16[208,256]{1,0:T(8,128)(2,1)}, bf16[208,256]{1,0:T(8,128)(2,1)S(1)}, u32[]{:S(2)}, u32[]{:S(2)}) collective-permute-start(bf16[208,256]{1,0:T(8,128)(2,1)} %get-tuple-element.35), channel_id=1, source_target_pairs={{0,4},{4,8},{8,12},{1,5},{5,9},{9,13},{2,6},{6,10},{10,14},{3,7},{... | collective-permute-start | bytes 319496 | tf_op jit(solution)/shard_map/ppermute | solution.py:23
  17.3 3.6 %collective-permute-start.2 = (bf16[208,256]{1,0:T(8,128)(2,1)}, bf16[208,256]{1,0:T(8,128)(2,1)S(1)}, u32[]{:S(2)}, u32[]{:S(2)}) collective-permute-start(bf16[208,256]{1,0:T(8,128)(2,1)} %get-tuple-element.35), channel_id=1, source_target_pairs={{0,8},{4,12},{1,9},{5,13},{2,10},{6,14},{3,11},{7,15},{16,24},{20,... | collective-permute-start | bytes 319496 | tf_op jit(solution)/shard_map/ppermute | solution.py:23
  26.0 6.6 %projected.3 = (bf16[128,2048]{1,0:T(8,128)(2,1)}, bf16[128,2048]{1,0:T(8,128)(2,1)}) custom-call(s32[1]{0:T(128)} %bitcast.order_ref, bf16[208,256]{1,0:T(8,128)(2,1)} %copy-done.20, bf16[208,256]{1,0:T(8,128)(2,1)} %copy-done.21, bf16[208,256]{1,0:T(8,128)(2,1)} %copy-done.22, f32[256,512]{1,0:T(8,128)} %near.3.refs_3_, ...), custom_call_target="tpu_custom_call" | custom-call | tf_op jit(solution)/shard_map/projected/pallas_call | solution.py:454
  33.4 6.3 %collective-permute-start.7 = (bf16[128,2048]{1,0:T(8,128)(2,1)}, bf16[128,2048]{1,0:T(8,128)(2,1)S(1)}, u32[]{:S(2)}, u32[]{:S(2)}) collective-permute-start(bf16[128,2048]{1,0:T(8,128)(2,1)} %get-tuple-element.46), channel_id=1, source_target_pairs={{0,1},{3,2},{4,5},{7,6},{8,9},{11,10},{12,13},{15,14},{16,17},{19,... | collective-permute-start | bytes 1572872 | tf_op jit(solution)/shard_map/ppermute | solution.py:667
  46.1 6.6 %projected.2 = (bf16[128,2048]{1,0:T(8,128)(2,1)}, bf16[128,2048]{1,0:T(8,128)(2,1)}) custom-call(s32[1]{0:T(128)} %bitcast.order_ref, bf16[208,256]{1,0:T(8,128)(2,1)} %copy-done.20, bf16[208,256]{1,0:T(8,128)(2,1)} %copy-done.21, bf16[208,256]{1,0:T(8,128)(2,1)} %copy-done.22, f32[256,512]{1,0:T(8,128)} %near.2.refs_3_, ...), custom_call_target="tpu_custom_call" | custom-call | tf_op jit(solution)/shard_map/projected/pallas_call | solution.py:454
  55.7 9.6 %collective-permute-done.4.one_ref = bf16[128,2048]{1,0:T(8,128)(2,1)S(1)} collective-permute-done((bf16[128,2048]{1,0:T(8,128)(2,1)}, bf16[128,2048]{1,0:T(8,128)(2,1)S(1)}, u32[]{:S(2)}, u32[]{:S(2)}) %collective-permute-start.4) | collective-permute-done | bytes 524320 | tf_op jit(solution)/shard_map/ppermute | solution.py:665
  65.4 8.8 %collective-permute-done.6.two_ref = bf16[128,2048]{1,0:T(8,128)(2,1)S(1)} collective-permute-done((bf16[128,2048]{1,0:T(8,128)(2,1)S(1)}, bf16[128,2048]{1,0:T(8,128)(2,1)S(1)}, u32[]{:S(2)}, u32[]{:S(2)}) %collective-permute-start.6) | collective-permute-done | bytes 524320 | tf_op jit(solution)/shard_map/ppermute | solution.py:668
  81.1 12.3 %collective-permute-done.10.refs_2_ = bf16[128,2176]{1,0:T(8,128)(2,1)} collective-permute-done((bf16[128,2176]{1,0:T(8,128)(2,1)}, bf16[128,2176]{1,0:T(8,128)(2,1)}, u32[]{:S(2)}, u32[]{:S(2)}) %collective-permute-start.10) | collective-permute-done | bytes 557088 | tf_op jit(solution)/shard_map/ppermute | solution.py:702
  94.1 11.6 %collective-permute-done.19.refs_0_ = bf16[128,2176]{1,0:T(8,128)(2,1)S(1)} collective-permute-done((bf16[128,2176]{1,0:T(8,128)(2,1)}, bf16[128,2176]{1,0:T(8,128)(2,1)S(1)}, u32[]{:S(2)}, u32[]{:S(2)}) %collective-permute-start.19) | collective-permute-done | bytes 557088 | tf_op jit(solution)/shard_map/ppermute | solution.py:703
  110.2 10.8 %collective-permute-done.31 = bf16[128,2176]{1,0:T(8,128)(2,1)S(1)} collective-permute-done((bf16[128,2176]{1,0:T(8,128)(2,1)S(1)}, bf16[128,2176]{1,0:T(8,128)(2,1)S(1)}, u32[]{:S(2)}, u32[]{:S(2)}) %collective-permute-start.31) | collective-permute-done | bytes 557088 | tf_op jit(solution)/shard_map/ppermute | solution.py:705
  124.3 11.4 %collective-permute-done.20.refs_1_ = bf16[128,2176]{1,0:T(8,128)(2,1)S(1)} collective-permute-done((bf16[128,2176]{1,0:T(8,128)(2,1)S(1)}, bf16[128,2176]{1,0:T(8,128)(2,1)S(1)}, u32[]{:S(2)}, u32[]{:S(2)}) %collective-permute-start.20) | collective-permute-done | bytes 557088 | tf_op jit(solution)/shard_map/ppermute | solution.py:528
  136.3 11.4 %collective-permute-done.32.refs_1_ = bf16[128,2176]{1,0:T(8,128)(2,1)S(1)} collective-permute-done((bf16[128,2176]{1,0:T(8,128)(2,1)S(1)}, bf16[128,2176]{1,0:T(8,128)(2,1)S(1)}, u32[]{:S(2)}, u32[]{:S(2)}) %collective-permute-start.32) | collective-permute-done | bytes 557088 | tf_op jit(solution)/shard_map/ppermute | solution.py:528
  147.7 10.4 %collective-permute-done.11.refs_3_ = bf16[128,2176]{1,0:T(8,128)(2,1)} collective-permute-done((bf16[128,2176]{1,0:T(8,128)(2,1)}, bf16[128,2176]{1,0:T(8,128)(2,1)}, u32[]{:S(2)}, u32[]{:S(2)}) %collective-permute-start.11) | collective-permute-done | bytes 557088 | tf_op jit(solution)/shard_map/ppermute | solution.py:528
  159.2 9.4 %expert.4 = (bf16[128,2048]{1,0:T(8,128)(2,1)}, bf16[128,2048]{1,0:T(8,128)(2,1)}, bf16[128,2048]{1,0:T(8,128)(2,1)}, bf16[128,2048]{1,0:T(8,128)(2,1)}) custom-call(s32[1]{0:T(128)} %bitcast.5.own_ref, bf16[128,2176]{1,0:T(8,128)(2,1)} %copy-done.1, bf16[128,2176]{1,0:T(8,128)(2,1)} %copy-done.3, bf16[128,2176]{1,0:T(8,128)(2,1)} %copy-done.5, ...), custom_call_target="tpu_custom_call" | custom-call | flops 3623878656 | bytes 12582912 | tf_op jit(solution)/shard_map/expert/pallas_call | solution.py:593
  169.0 9.5 %expert.5 = (bf16[128,2048]{1,0:T(8,128)(2,1)}, bf16[128,2048]{1,0:T(8,128)(2,1)}, bf16[128,2048]{1,0:T(8,128)(2,1)}, bf16[128,2048]{1,0:T(8,128)(2,1)}) custom-call(s32[1]{0:T(128)} %bitcast.5.own_ref, bf16[128,2176]{1,0:T(8,128)(2,1)} %copy-done, bf16[128,2176]{1,0:T(8,128)(2,1)} %copy-done.2, bf16[128,2176]{1,0:T(8,128)(2,1)} %copy-done.4, ...), custom_call_target="tpu_custom_call" | custom-call | flops 3623878656 | bytes 12582912 | tf_op jit(solution)/shard_map/expert/pallas_call | solution.py:593
  178.8 14.7 %expert.3 = (bf16[128,2048]{1,0:T(8,128)(2,1)}, bf16[128,2048]{1,0:T(8,128)(2,1)}, bf16[128,2048]{1,0:T(8,128)(2,1)}, bf16[128,2048]{1,0:T(8,128)(2,1)}, bf16[12...) custom-call(s32[1]{0:T(128)} %bitcast.5.own_ref, ...), custom_call_target="tpu_custom_call" | custom-call | flops 7247757312 | bytes 12582912 | tf_op jit(solution)/shard_map/expert/pallas_call | solution.py:593
  202.2 8.1 %collective-permute-done.37 = bf16[128,2048]{1,0:T(8,128)(2,1)} collective-permute-done((bf16[128,2048]{1,0:T(8,128)(2,1)}, bf16[128,2048]{1,0:T(8,128)(2,1)}, u32[]{:S(2)}, u32[]{:S(2)}) %collective-permute-start.37) | collective-permute-done | bytes 524320 | tf_op jit(solution)/shard_map/ppermute | solution.py:528
  214.2 7.2 %collective-permute-done.25 = bf16[128,2048]{1,0:T(8,128)(2,1)} collective-permute-done((bf16[128,2048]{1,0:T(8,128)(2,1)S(1)}, bf16[128,2048]{1,0:T(8,128)(2,1)}, u32[]{:S(2)}, u32[]{:S(2)}) %collective-permute-start.25) | collective-permute-done | bytes 524320 | tf_op jit(solution)/shard_map/ppermute | solution.py:528
  221.5 4.3 %collective-permute-start.40 = (bf16[128,2048]{1,0:T(8,128)(2,1)S(1)}, bf16[128,2048]{1,0:T(8,128)(2,1)S(1)}, u32[]{:S(2)}, u32[]{:S(2)}) collective-permute-start(bf16[128,2048]{1,0:T(8,128)(2,1)S(1)} %add.51), channel_id=1, source_target_pairs={{0,1},{3,2},{4,5},{7,6},{8,9},{11,10},{12,13},{15,14},{16,17},{19,... | collective-permute-start | bytes 1572872 | tf_op jit(solution)/shard_map/ppermute | solution.py:667
  232.6 3.4 %collective-permute-start.26 = (bf16[128,2048]{1,0:T(8,128)(2,1)S(1)}, bf16[128,2048]{1,0:T(8,128)(2,1)S(1)}, u32[]{:S(2)}, u32[]{:S(2)}) collective-permute-start(bf16[128,2048]{1,0:T(8,128)(2,1)S(1)} %add_convert_fusion.1), channel_id=1, source_target_pairs={{0,3},{3,0},{4,7},{7,4},{8,11},{11,8},{12,15},{15,12},{16,19},{19,... | collective-permute-start | bytes 1572872 | tf_op jit(solution)/shard_map/ppermute | solution.py:665
  237.7 5.5 %collective-permute-done.18.refs_2_ = bf16[128,2048]{1,0:T(8,128)(2,1)S(1)} collective-permute-done((bf16[128,2048]{1,0:T(8,128)(2,1)S(1)}, bf16[128,2048]{1,0:T(8,128)(2,1)S(1)}, u32[]{:S(2)}, u32[]{:S(2)}) %collective-permute-start.18) | collective-permute-done | bytes 524320 | tf_op jit(solution)/shard_map/ppermute | solution.py:528
  243.1 8.0 %collective-permute-done.26.refs_3_ = bf16[128,2048]{1,0:T(8,128)(2,1)S(1)} collective-permute-done((bf16[128,2048]{1,0:T(8,128)(2,1)S(1)}, bf16[128,2048]{1,0:T(8,128)(2,1)S(1)}, u32[]{:S(2)}, u32[]{:S(2)}) %collective-permute-start.26) | collective-permute-done | bytes 524320 | tf_op jit(solution)/shard_map/ppermute | solution.py:665
  251.2 8.8 %collective-permute-done.39.refs_4_ = bf16[128,2048]{1,0:T(8,128)(2,1)S(1)} collective-permute-done((bf16[128,2048]{1,0:T(8,128)(2,1)S(1)}, bf16[128,2048]{1,0:T(8,128)(2,1)S(1)}, u32[]{:S(2)}, u32[]{:S(2)}) %collective-permute-start.39) | collective-permute-done | bytes 524320 | tf_op jit(solution)/shard_map/ppermute | solution.py:668
  (146 shorter events, 63.6 us)
Async XLA Ops:
  32.6 20.2 %collective-permute-start.5 = (bf16[128,2048]{1,0:T(8,128)(2,1)}, bf16[128,2048]{1,0:T(8,128)(2,1)S(1)}, u32[]{:S(2)}, u32[]{:S(2)}) collective-permute-start(bf16[128,2048]{1,0:T(8,128)(2,1)} %get-tuple-element.46), channel_id=1, source_target_pairs={{1,2},{2,1},{5,6},{6,5},{9,10},{10,9},{13,14},{14,13},{17,18},{18,... | collective-permute-start | bytes 1572872 | tf_op jit(solution)/shard_map/ppermute | solution.py:666
  33.4 20.6 %collective-permute-start.7 = (bf16[128,2048]{1,0:T(8,128)(2,1)}, bf16[128,2048]{1,0:T(8,128)(2,1)S(1)}, u32[]{:S(2)}, u32[]{:S(2)}) collective-permute-start(bf16[128,2048]{1,0:T(8,128)(2,1)} %get-tuple-element.46), channel_id=1, source_target_pairs={{0,1},{3,2},{4,5},{7,6},{8,9},{11,10},{12,13},{15,14},{16,17},{19,... | collective-permute-start | bytes 1572872 | tf_op jit(solution)/shard_map/ppermute | solution.py:667
  42.7 22.6 %collective-permute-start.4 = (bf16[128,2048]{1,0:T(8,128)(2,1)}, bf16[128,2048]{1,0:T(8,128)(2,1)S(1)}, u32[]{:S(2)}, u32[]{:S(2)}) collective-permute-start(bf16[128,2048]{1,0:T(8,128)(2,1)} %get-tuple-element.44), channel_id=1, source_target_pairs={{0,3},{3,0},{4,7},{7,4},{8,11},{11,8},{12,15},{15,12},{16,19},{19,... | collective-permute-start | bytes 1572872 | tf_op jit(solution)/shard_map/ppermute | solution.py:665
  54.0 20.2 %collective-permute-start.6 = (bf16[128,2048]{1,0:T(8,128)(2,1)S(1)}, bf16[128,2048]{1,0:T(8,128)(2,1)S(1)}, u32[]{:S(2)}, u32[]{:S(2)}) collective-permute-start(bf16[128,2048]{1,0:T(8,128)(2,1)S(1)} %add.41), channel_id=1, source_target_pairs={{0,1},{1,0},{2,3},{3,2},{4,5},{5,4},{6,7},{7,6},{8,9},{9,8},{10,11... | collective-permute-start | bytes 1572872 | tf_op jit(solution)/shard_map/ppermute | solution.py:668
  78.9 26.8 %collective-permute-start.19 = (bf16[128,2176]{1,0:T(8,128)(2,1)}, bf16[128,2176]{1,0:T(8,128)(2,1)S(1)}, u32[]{:S(2)}, u32[]{:S(2)}) collective-permute-start(bf16[128,2176]{1,0:T(8,128)(2,1)} %get-tuple-element.48.refs_0_), channel_id=1, source_target_pairs={{1,2},{2,1},{0,3},{3,0},{5,6},{6,5},{4,7},{7,4},{9,10},{10,9},{8,1... | collective-permute-start | bytes 1671176 | tf_op jit(solution)/shard_map/ppermute | solution.py:703
  107.2 28.6 %collective-permute-start.9 = (bf16[128,2176]{1,0:T(8,128)(2,1)}, bf16[128,2176]{1,0:T(8,128)(2,1)S(1)}, u32[]{:S(2)}, u32[]{:S(2)}) collective-permute-start(bf16[128,2176]{1,0:T(8,128)(2,1)} %get-tuple-element.48.refs_0_), channel_id=1, source_target_pairs={{0,8},{4,12},{8,0},{12,4},{1,9},{5,13},{9,1},{13,5},{2,10},{6,14},... | collective-permute-start | bytes 1671176 | tf_op jit(solution)/shard_map/ppermute | solution.py:528
  110.1 25.6 %collective-permute-start.20 = (bf16[128,2176]{1,0:T(8,128)(2,1)S(1)}, bf16[128,2176]{1,0:T(8,128)(2,1)S(1)}, u32[]{:S(2)}, u32[]{:S(2)}) collective-permute-start(bf16[128,2176]{1,0:T(8,128)(2,1)S(1)} %collective-permute-done.19.refs_0_), channel_id=1, source_target_pairs={{0,8},{4,12},{8,0},{12,4},{1,9},{5,13},{9,1},{13,5},{2,10},{6,14},... | collective-permute-start | bytes 1671176 | tf_op jit(solution)/shard_map/ppermute | solution.py:528
  121.1 26.6 %collective-permute-start.32 = (bf16[128,2176]{1,0:T(8,128)(2,1)S(1)}, bf16[128,2176]{1,0:T(8,128)(2,1)S(1)}, u32[]{:S(2)}, u32[]{:S(2)}) collective-permute-start(bf16[128,2176]{1,0:T(8,128)(2,1)S(1)} %broadcast_select_fusion.refs_0_), channel_id=1, source_target_pairs={{0,8},{4,12},{8,0},{12,4},{1,9},{5,13},{9,1},{13,5},{2,10},{6,14},... | collective-permute-start | bytes 1671176 | tf_op jit(solution)/shard_map/ppermute | solution.py:528
  124.3 33.9 %collective-permute-start.11 = (bf16[128,2176]{1,0:T(8,128)(2,1)}, bf16[128,2176]{1,0:T(8,128)(2,1)}, u32[]{:S(2)}, u32[]{:S(2)}) collective-permute-start(bf16[128,2176]{1,0:T(8,128)(2,1)} %collective-permute-done.10.refs_2_), channel_id=1, source_target_pairs={{0,8},{4,12},{8,0},{12,4},{1,9},{5,13},{9,1},{13,5},{2,10},{6,14},... | collective-permute-start | bytes 1671176 | tf_op jit(solution)/shard_map/ppermute | solution.py:528
  124.3 33.8 %collective-permute-start.21 = (bf16[128,2176]{1,0:T(8,128)(2,1)S(1)}, bf16[128,2176]{1,0:T(8,128)(2,1)S(1)}, u32[]{:S(2)}, u32[]{:S(2)}) collective-permute-start(bf16[128,2176]{1,0:T(8,128)(2,1)S(1)} %collective-permute-done.19.refs_0_), channel_id=1, source_target_pairs={{0,4},{4,0},{8,12},{12,8},{1,5},{5,1},{9,13},{13,9},{2,6},{6,2},{1... | collective-permute-start | bytes 1671176 | tf_op jit(solution)/shard_map/ppermute | solution.py:528
  135.8 22.9 %collective-permute-start.22 = (bf16[128,2176]{1,0:T(8,128)(2,1)S(1)}, bf16[128,2176]{1,0:T(8,128)(2,1)}, u32[]{:S(2)}, u32[]{:S(2)}) collective-permute-start(bf16[128,2176]{1,0:T(8,128)(2,1)S(1)} %collective-permute-done.20.refs_1_), channel_id=1, source_target_pairs={{0,4},{4,0},{8,12},{12,8},{1,5},{5,1},{9,13},{13,9},{2,6},{6,2},{1... | collective-permute-start | bytes 1671176 | tf_op jit(solution)/shard_map/ppermute | solution.py:528
  135.8 23.0 %collective-permute-start.33 = (bf16[128,2176]{1,0:T(8,128)(2,1)S(1)}, bf16[128,2176]{1,0:T(8,128)(2,1)S(1)}, u32[]{:S(2)}, u32[]{:S(2)}) collective-permute-start(bf16[128,2176]{1,0:T(8,128)(2,1)S(1)} %broadcast_select_fusion.refs_0_), channel_id=1, source_target_pairs={{0,4},{4,0},{8,12},{12,8},{1,5},{5,1},{9,13},{13,9},{2,6},{6,2},{1... | collective-permute-start | bytes 1671176 | tf_op jit(solution)/shard_map/ppermute | solution.py:528
  147.7 20.9 %collective-permute-start.34 = (bf16[128,2176]{1,0:T(8,128)(2,1)S(1)}, bf16[128,2176]{1,0:T(8,128)(2,1)}, u32[]{:S(2)}, u32[]{:S(2)}) collective-permute-start(bf16[128,2176]{1,0:T(8,128)(2,1)S(1)} %collective-permute-done.32.refs_1_), channel_id=1, source_target_pairs={{0,4},{4,0},{8,12},{12,8},{1,5},{5,1},{9,13},{13,9},{2,6},{6,2},{1... | collective-permute-start | bytes 1671176 | tf_op jit(solution)/shard_map/ppermute | solution.py:528
  158.2 20.3 %collective-permute-start.12 = (bf16[128,2176]{1,0:T(8,128)(2,1)}, bf16[128,2176]{1,0:T(8,128)(2,1)}, u32[]{:S(2)}, u32[]{:S(2)}) collective-permute-start(bf16[128,2176]{1,0:T(8,128)(2,1)} %get-tuple-element.48.refs_0_), channel_id=1, source_target_pairs={{0,4},{4,0},{8,12},{12,8},{1,5},{5,1},{9,13},{13,9},{2,6},{6,2},{1... | collective-permute-start | bytes 1671176 | tf_op jit(solution)/shard_map/ppermute | solution.py:528
  158.2 20.7 %collective-permute-start.14 = (bf16[128,2176]{1,0:T(8,128)(2,1)}, bf16[128,2176]{1,0:T(8,128)(2,1)}, u32[]{:S(2)}, u32[]{:S(2)}) collective-permute-start(bf16[128,2176]{1,0:T(8,128)(2,1)} %collective-permute-done.10.refs_2_), channel_id=1, source_target_pairs={{0,4},{4,0},{8,12},{12,8},{1,5},{5,1},{9,13},{13,9},{2,6},{6,2},{1... | collective-permute-start | bytes 1671176 | tf_op jit(solution)/shard_map/ppermute | solution.py:528
  158.7 20.1 %collective-permute-start.13 = (bf16[128,2176]{1,0:T(8,128)(2,1)}, bf16[128,2176]{1,0:T(8,128)(2,1)}, u32[]{:S(2)}, u32[]{:S(2)}) collective-permute-start(bf16[128,2176]{1,0:T(8,128)(2,1)} %copy-done.25), channel_id=1, source_target_pairs={{0,4},{4,0},{8,12},{12,8},{1,5},{5,1},{9,13},{13,9},{2,6},{6,2},{1... | collective-permute-start | bytes 1671176 | tf_op jit(solution)/shard_map/ppermute | solution.py:528
  168.7 28.2 %collective-permute-start.24 = (bf16[128,2048]{1,0:T(8,128)(2,1)}, bf16[128,2048]{1,0:T(8,128)(2,1)S(1)}, u32[]{:S(2)}, u32[]{:S(2)}) collective-permute-start(bf16[128,2048]{1,0:T(8,128)(2,1)} %get-tuple-element.56), channel_id=1, source_target_pairs={{0,4},{4,0},{8,12},{12,8},{1,5},{5,1},{9,13},{13,9},{2,6},{6,2},{1... | collective-permute-start | bytes 1572872 | tf_op jit(solution)/shard_map/ppermute | solution.py:528
  197.5 23.9 %collective-permute-start.25 = (bf16[128,2048]{1,0:T(8,128)(2,1)S(1)}, bf16[128,2048]{1,0:T(8,128)(2,1)}, u32[]{:S(2)}, u32[]{:S(2)}) collective-permute-start(bf16[128,2048]{1,0:T(8,128)(2,1)S(1)} %add.45), channel_id=1, source_target_pairs={{0,8},{4,12},{8,0},{12,4},{1,9},{5,13},{9,1},{13,5},{2,10},{6,14},... | collective-permute-start | bytes 1572872 | tf_op jit(solution)/shard_map/ppermute | solution.py:528
  200.0 27.4 %collective-permute-start.27 = (bf16[128,2048]{1,0:T(8,128)(2,1)}, bf16[128,2048]{1,0:T(8,128)(2,1)S(1)}, u32[]{:S(2)}, u32[]{:S(2)}) collective-permute-start(bf16[128,2048]{1,0:T(8,128)(2,1)} %get-tuple-element.58), channel_id=1, source_target_pairs={{0,4},{4,0},{8,12},{12,8},{1,5},{5,1},{9,13},{13,9},{2,6},{6,2},{1... | collective-permute-start | bytes 1572872 | tf_op jit(solution)/shard_map/ppermute | solution.py:528
  210.2 22.4 %collective-permute-start.29 = (bf16[128,2048]{1,0:T(8,128)(2,1)S(1)}, bf16[128,2048]{1,0:T(8,128)(2,1)S(1)}, u32[]{:S(2)}, u32[]{:S(2)}) collective-permute-start(bf16[128,2048]{1,0:T(8,128)(2,1)S(1)} %add.48), channel_id=1, source_target_pairs={{0,8},{4,12},{8,0},{12,4},{1,9},{5,13},{9,1},{13,5},{2,10},{6,14},... | collective-permute-start | bytes 1572872 | tf_op jit(solution)/shard_map/ppermute | solution.py:528
  213.3 22.7 %collective-permute-start.38 = (bf16[128,2048]{1,0:T(8,128)(2,1)S(1)}, bf16[128,2048]{1,0:T(8,128)(2,1)S(1)}, u32[]{:S(2)}, u32[]{:S(2)}) collective-permute-start(bf16[128,2048]{1,0:T(8,128)(2,1)S(1)} %add.51), channel_id=1, source_target_pairs={{1,2},{2,1},{5,6},{6,5},{9,10},{10,9},{13,14},{14,13},{17,18},{18,... | collective-permute-start | bytes 1572872 | tf_op jit(solution)/shard_map/ppermute | solution.py:666
  214.2 23.5 %collective-permute-start.16 = (bf16[128,2048]{1,0:T(8,128)(2,1)}, bf16[128,2048]{1,0:T(8,128)(2,1)S(1)}, u32[]{:S(2)}, u32[]{:S(2)}) collective-permute-start(bf16[128,2048]{1,0:T(8,128)(2,1)} %get-tuple-element.50), channel_id=1, source_target_pairs={{0,4},{4,0},{8,12},{12,8},{1,5},{5,1},{9,13},{13,9},{2,6},{6,2},{1... | collective-permute-start | bytes 1572872 | tf_op jit(solution)/shard_map/ppermute | solution.py:528
  236.4 23.6 %collective-permute-start.39 = (bf16[128,2048]{1,0:T(8,128)(2,1)S(1)}, bf16[128,2048]{1,0:T(8,128)(2,1)S(1)}, u32[]{:S(2)}, u32[]{:S(2)}) collective-permute-start(bf16[128,2048]{1,0:T(8,128)(2,1)S(1)} %fusion), channel_id=1, source_target_pairs={{0,1},{1,0},{2,3},{3,2},{4,5},{5,4},{6,7},{7,6},{8,9},{9,8},{10,11... | collective-permute-start | bytes 1572872 | tf_op jit(solution)/shard_map/ppermute | solution.py:668
  236.9 23.0 %collective-permute-start.41 = (bf16[128,2048]{1,0:T(8,128)(2,1)S(1)}, bf16[128,2048]{1,0:T(8,128)(2,1)S(1)}, u32[]{:S(2)}, u32[]{:S(2)}) collective-permute-start(bf16[128,2048]{1,0:T(8,128)(2,1)S(1)} %add.53), channel_id=1, source_target_pairs={{1,2},{2,1},{5,6},{6,5},{9,10},{10,9},{13,14},{14,13},{17,18},{18,... | collective-permute-start | bytes 1572872 | tf_op jit(solution)/shard_map/ppermute | solution.py:669
  (45 other events, 610.2 us)
